TPU v7x, 256 devices: a 4x2x16 block of a 4x16x16 slice. The times are simulated.
256 devices in a mesh: grp: 2 (over y), sp: 32 (over z, core), tp: 4 (over x).
Axes of the slice: x: 4, y: 2, z: 16, core: 2. Of those that a mesh axis runs over, the one named last changes fastest.
The devices are a block of a 4x16x16 slice.
Arguments:
- residual: bfloat16 [16384, 2048], P(('grp', 'sp', 'tp')), parts along dimension 0, may hold values from -6 to 6
- queries_wide: bfloat16 [16384, 1024], P(('grp', 'sp'), 'tp'), parts along dimension 0, may hold values from -6 to 6
- keys_wide: bfloat16 [16384, 512], P(('grp', 'sp'), 'tp'), parts along dimension 0, may hold values from -6 to 6
- values_wide: bfloat16 [16384, 512], P(('grp', 'sp'), 'tp'), parts along dimension 0, may hold values from -6 to 6
- queries_narrow: bfloat16 [16384, 512], P(('grp', 'sp'), 'tp'), parts along dimension 0, may hold values from -6 to 6
- keys_narrow: bfloat16 [16384, 256], P(('grp', 'sp'), 'tp'), parts along dimension 0, may hold values from -6 to 6
- values_narrow: bfloat16 [16384, 256], P(('grp', 'sp'), 'tp'), parts along dimension 0, may hold values from -6 to 6
- query_gain_wide: float32 [128], replicated, may hold values from 1 to 6
- key_gain_wide: float32 [128], replicated, may hold values from 1 to 6
- query_gain_narrow: float32 [64], replicated, may hold values from 1 to 6
- key_gain_narrow: float32 [64], replicated, may hold values from 1 to 6
- output_wide: bfloat16 [1024, 2048], P('tp'), may hold values from -0.3125 to 0.3125
- output_narrow: bfloat16 [512, 2048], P('tp'), may hold values from -0.3125 to 0.3125
- norm_gain: float32 [2048], replicated, may hold values from 0.1 to 1.9
- gate_weight: bfloat16 [32, 2048, 3584], P('sp', None, 'tp'), may hold values from -0.125 to 0.125
- up_weight: bfloat16 [32, 2048, 3584], P('sp', None, 'tp'), may hold values from -0.125 to 0.125
- down_weight: bfloat16 [32, 3584, 2048], P('sp', 'tp'), may hold values from -0.09375 to 0.09375
- route_ids: int32 [16384, 2], P(('grp', 'sp', 'tp')), parts along dimension 0, may hold values from 0 to 31, all different within a row; in each aligned block of 64 rows (0 to 63, 64 to 127, ...) at most 8 rows name the same one
- route_weights: float32 [16384, 2], P(('grp', 'sp', 'tp')), parts along dimension 0, may hold values from 0.1 to 0.9
Outputs:
- result: bfloat16 [16384, 2048], P(('grp', 'sp', 'tp')), parts along dimension 0
There are 2 independent parts, one for each index of `grp`. A program takes and returns all parts, laid end to end along the dimension named above; an argument that names none is the same for every part. Nothing has to cross between parts.
Inputs may be any that keep to these rules, and one draw needn't show every extreme that they name: `route_ids`: in each aligned block of 64 rows (the rows of one device) no expert is named by more than 8 rows, a bound that some block reaches; a row names 2 different experts.
All inputs are finite; a program needn't handle non-finite values.
Results may differ from a plain program's by a relative error of at most 0.013.
The roundings to bfloat16 on the way count: a program that leaves them out, or rounds other values in their place, can miss the bound.
Values may be sent and summed in bfloat16 or wider, within the bound.
A program may use at most 128 MiB of HBM per device.

v0:
```python
import jax
import jax.numpy as jnp
from jax import lax
from jax.sharding import PartitionSpec as P

GRID = 64


THETA = 10000.0
EPS = 1e-06
NEG_BIG = -1e30


def sent_together(arrays, axis, dim, along):
    both = jnp.concatenate(arrays, axis=along)
    out, at, finished = (lax.all_gather(both, axis, axis=dim, tiled=True), 0, [])
    for a in arrays:
        finished.append(lax.slice_in_dim(out, at, at + a.shape[along], axis=along))
        at += a.shape[along]
    return tuple(finished)


def in_blocks(value, dim, peers):
    lengths = value.shape
    blocks = value.reshape(*lengths[:dim], peers, lengths[dim] // peers, *lengths[dim + 1 :])
    return jnp.moveaxis(blocks, dim, 0)


def sum_at_owner(value, axis, dim):
    peers = lax.axis_size(axis)
    blocks = lax.all_to_all(in_blocks(value, dim, peers), axis, 0, 0, tiled=True)
    return jnp.sum(blocks.astype(jnp.float32), axis=0)


def items_in_groups(value, axis, split_dim, concat_dim, work, item_dim, out_dim):
    items = jax.tree.leaves(value)[0].shape[item_dim]
    count = 2 if items % 2 == 0 else 1
    finished = []
    for k in range(count):
        group = jax.tree.map(
            lambda a: lax.slice_in_dim(
                a, k * (items // count), (k + 1) * (items // count), axis=item_dim
            ),
            value,
        )
        finished.append(
            work(
                lax.all_to_all(
                    group, axis, split_axis=split_dim, concat_axis=concat_dim, tiled=True
                )
            )
        )
    return jax.tree.map(lambda *parts: jnp.concatenate(parts, axis=out_dim), *finished)


def rotary_tables(places, head_width):
    quarter = head_width // 4
    inv_freq = THETA ** (-jnp.arange(quarter, dtype=jnp.float32) / quarter)
    grid_rows = (places // GRID).astype(jnp.float32)
    grid_cols = (places % GRID).astype(jnp.float32)
    row_angle = grid_rows[:, None] * inv_freq[None, :]
    col_angle = grid_cols[:, None] * inv_freq[None, :]
    angles = jnp.concatenate([row_angle, row_angle, col_angle, col_angle], axis=-1)
    return (jnp.cos(angles), jnp.sin(angles))


def head_norm_rotate(values, gain_vec, cos_table, sin_table):
    as_float = values.astype(jnp.float32)
    scaled = as_float * lax.rsqrt(jnp.mean(as_float * as_float, axis=-1, keepdims=True) + EPS)
    scaled = scaled * gain_vec
    full_shape = scaled.shape
    quarter = full_shape[-1] // 4
    halves = scaled.reshape(full_shape[:-1] + (2, 2, quarter))
    turned = jnp.stack([-halves[..., 1, :], halves[..., 0, :]], axis=-2).reshape(full_shape)
    return (scaled * cos_table[:, None, :] + turned * sin_table[:, None, :]).astype(jnp.bfloat16)


def fresh_state(queries):
    key_heads, group_size, tok_count = (queries.shape[1], queries.shape[2], queries.shape[0])
    return (
        jnp.full((key_heads, group_size, tok_count), NEG_BIG, jnp.float32),
        jnp.zeros((key_heads, group_size, tok_count), jnp.float32),
        jnp.zeros(queries.shape, jnp.float32),
    )


def key_sweep(carried, queries, keys, values):
    key_count = keys.shape[0]
    key_heads = queries.shape[1]
    head_width = queries.shape[3]
    block_len = 2048
    key_blocks = keys.reshape(key_count // block_len, block_len, key_heads, head_width)
    value_blocks = values.reshape(key_count // block_len, block_len, key_heads, head_width)
    score_scale = head_width ** (-0.5)

    def step(carried_state, blocks_in):
        key_block, value_block = blocks_in
        running_max, weight_sum, weighted = carried_state
        scores = (
            jnp.einsum("qhgd,khd->hgqk", queries, key_block, preferred_element_type=jnp.float32)
            * score_scale
        )
        new_max = jnp.maximum(running_max, jnp.max(scores, axis=-1))
        weights = jnp.exp(scores - new_max[..., None])
        rescale = jnp.exp(running_max - new_max)
        weight_sum = weight_sum * rescale + jnp.sum(weights, axis=-1)
        mixed_values = jnp.einsum(
            "hgqk,khd->qhgd",
            weights.astype(jnp.bfloat16),
            value_block,
            preferred_element_type=jnp.float32,
        )
        weighted = weighted * jnp.transpose(rescale, (2, 0, 1))[..., None] + mixed_values
        return ((new_max, weight_sum, weighted), None)

    carried, _ = lax.scan(step, carried, (key_blocks, value_blocks))
    return carried


def finish_heads(carried):
    weighted = carried[2]
    outcome = weighted / jnp.transpose(carried[1], (2, 0, 1))[..., None]
    return outcome.astype(jnp.bfloat16).reshape(weighted.shape[0], -1)


def slot_tables(chosen, slot_count, expert_count):
    row_count = chosen.shape[0]
    pick_count = chosen.shape[1]
    flat_pick = chosen.reshape(row_count * pick_count)
    hit_marks = (flat_pick[:, None] == jnp.arange(expert_count, dtype=jnp.int32)[None, :]).astype(
        jnp.int32
    )
    before = jnp.cumsum(hit_marks, axis=0) - hit_marks
    slot_place = jnp.sum(before * hit_marks, axis=1)
    target = flat_pick * slot_count + slot_place
    slot_table = target[:, None] == jnp.arange(expert_count * slot_count, dtype=jnp.int32)[None, :]
    return slot_table.astype(jnp.bfloat16).reshape(row_count, pick_count, expert_count * slot_count)


def body(
    residual,
    queries_wide,
    keys_wide,
    values_wide,
    queries_narrow,
    keys_narrow,
    values_narrow,
    query_gain_wide,
    key_gain_wide,
    query_gain_narrow,
    key_gain_narrow,
    output_wide,
    output_narrow,
    norm_gain,
    gate_weight,
    up_weight,
    down_weight,
    route_ids,
    route_weights,
):
    tok_count = queries_wide.shape[0]
    places = lax.axis_index("sp") * tok_count + jnp.arange(tok_count, dtype=jnp.int32)
    wide_width = query_gain_wide.shape[0]
    narrow_width = query_gain_narrow.shape[0]
    cos_wide, sin_wide = rotary_tables(places, wide_width)
    cos_narrow, sin_narrow = rotary_tables(places, narrow_width)
    wide_keyheads = keys_wide.shape[1] // wide_width
    narrow_keyheads = keys_narrow.shape[1] // narrow_width
    q_wide = head_norm_rotate(
        queries_wide.reshape(tok_count, -1, wide_width), query_gain_wide, cos_wide, sin_wide
    )
    q_wide = q_wide.reshape(tok_count, wide_keyheads, -1, wide_width)
    k_wide = head_norm_rotate(
        keys_wide.reshape(tok_count, -1, wide_width), key_gain_wide, cos_wide, sin_wide
    )
    k_wide = k_wide.reshape(tok_count, -1)
    q_narrow = head_norm_rotate(
        queries_narrow.reshape(tok_count, -1, narrow_width),
        query_gain_narrow,
        cos_narrow,
        sin_narrow,
    )
    q_narrow = q_narrow.reshape(tok_count, narrow_keyheads, -1, narrow_width)
    k_narrow = head_norm_rotate(
        keys_narrow.reshape(tok_count, -1, narrow_width), key_gain_narrow, cos_narrow, sin_narrow
    )
    k_narrow = k_narrow.reshape(tok_count, -1)
    carried = (fresh_state(q_wide), fresh_state(q_narrow))
    pieces = sent_together((k_wide, values_wide, k_narrow, values_narrow), "sp", 0, 1)
    carried = (
        key_sweep(carried[0], q_wide, pieces[0], pieces[1]),
        key_sweep(carried[1], q_narrow, pieces[2], pieces[3]),
    )
    heads_wide = finish_heads(carried[0])
    heads_narrow = finish_heads(carried[1])
    own_rows = residual.shape[0]
    mixed_heads = sum_at_owner(
        (
            jnp.dot(heads_wide, output_wide, preferred_element_type=jnp.float32)
            + jnp.dot(heads_narrow, output_narrow, preferred_element_type=jnp.float32)
        ).astype(jnp.bfloat16),
        "tp",
        0,
    )
    attended = (residual.astype(jnp.float32) + mixed_heads).astype(jnp.bfloat16)
    state_float = attended.astype(jnp.float32)
    normed = (
        state_float
        * lax.rsqrt(jnp.mean(state_float * state_float, axis=-1, keepdims=True) + EPS)
        * norm_gain
    ).astype(jnp.bfloat16)
    pick_count = route_ids.shape[1]
    expert_count = lax.axis_size("sp")
    slot_count = 2 * pick_count * own_rows // expert_count
    model_width = residual.shape[1]
    own_tables = slot_tables(route_ids, slot_count, expert_count)

    def expert_block(arrived):
        full_shape = arrived.shape
        flat_rows = arrived.reshape(-1, model_width)
        gate_act = jnp.dot(flat_rows, gate_weight[0], preferred_element_type=jnp.float32)
        up_act = jnp.dot(flat_rows, up_weight[0], preferred_element_type=jnp.float32)
        hidden = (jax.nn.silu(gate_act) * up_act).astype(jnp.bfloat16)
        partial_value = jnp.dot(hidden, down_weight[0], preferred_element_type=jnp.float32).reshape(
            full_shape
        )
        summed = sum_at_owner(partial_value.astype(jnp.bfloat16), "tp", 0)
        return summed.reshape(full_shape[1:]).astype(jnp.bfloat16)

    send_rows = jnp.einsum(
        "rks,rd->sd", own_tables, normed, preferred_element_type=jnp.float32
    ).astype(jnp.bfloat16)
    send_rows = send_rows.reshape(expert_count, slot_count, model_width)

    def copy_then_run(arrived):
        copies = lax.all_gather(arrived, "tp", axis=0, tiled=True)
        return expert_block(copies.reshape((lax.axis_size("tp"),) + arrived.shape))

    results = items_in_groups(send_rows, "sp", 0, 0, copy_then_run, 1, 1)
    returned = lax.all_to_all(results, "sp", split_axis=0, concat_axis=0, tiled=True)
    returned_flat = returned.reshape(expert_count * slot_count, model_width)
    picked = jnp.einsum(
        "rks,sd->rkd", own_tables, returned_flat, preferred_element_type=jnp.float32
    )
    mixture = jnp.sum(route_weights[:, :, None] * picked, axis=1)
    return (state_float + mixture).astype(jnp.bfloat16)


def solution(mesh):
    return jax.shard_map(
        body,
        mesh=mesh,
        in_specs=(
            P(("grp", "sp", "tp"), None),
            P(("grp", "sp"), "tp"),
            P(("grp", "sp"), "tp"),
            P(("grp", "sp"), "tp"),
            P(("grp", "sp"), "tp"),
            P(("grp", "sp"), "tp"),
            P(("grp", "sp"), "tp"),
            P(),
            P(),
            P(),
            P(),
            P("tp", None),
            P("tp", None),
            P(),
            P("sp", None, "tp"),
            P("sp", None, "tp"),
            P("sp", "tp", None),
            P(("grp", "sp", "tp"), None),
            P(("grp", "sp", "tp"), None),
        ),
        out_specs=P(("grp", "sp", "tp"), None),
        check_vma=False,
    )
```

profile of v0, /device:TPU:33, one launch (start us, length us, event | category | flops | bytes accessed | tf_op | source)
XLA Modules:
  0.0 469.3 jit_solution(13524277643561501845)
XLA Ops:
  15.1 98.7 %all-gather.4.cloned.1.call-done = bf16[8192,384]{0,1:T(8,128)(2,1)} async-done(((bf16[256,384]{0,1:T(8,128)(2,1)}), bf16[8192,384]{0,1:T(8,128)(2,1)}) %all-gather.4.cloned.1.call-update) | async-done | bytes 6291472 | tf_op jit(solution)/shard_map/all_gather | solution.py:16
  122.4 34.8 %while.31 = (s32[]{:T(128)}, f32[1,2,256]{2,1,0:T(2,128)S(1)}, f32[1,2,256]{2,1,0:T(2,128)}, f32[256,1,2,64]{0,3,2,1:T(8,128)}, bf16[4,2048,1,64]{1,3,2,0:T(8,12...) while((s32[]{:T(128)}, f32[1,2,256]{2,1,0:T(2,128)S(1)}, ...), condition=%wide.region_11.12_spmd.clone, body=%wide.region_8.11_spmd.clone.sunk | while | flops 276925440 | bytes 30261444 | solution.py:116
  122.4 3.6 bitcast_reduce_fusion.9
  126.0 3.8 fusion.139
  131.1 3.6 bitcast_reduce_fusion.9
  134.7 3.8 fusion.139
  139.8 3.6 bitcast_reduce_fusion.9
  143.4 3.8 fusion.139
  148.5 3.6 bitcast_reduce_fusion.9
  152.1 3.8 fusion.139
  157.2 4.7 fusion.108
  161.9 3.2 copy.145
  165.1 4.1 copy.126
  169.2 28.0 %while.30 = (s32[]{:T(128)}, f32[1,2,256]{2,1,0:T(2,128)S(1)}, f32[1,2,256]{2,1,0:T(2,128)S(1)}, f32[256,1,2,128]{0,3,2,1:T(8,128)S(1)}, bf16[4,2048,1,128]{3,1,...) while((s32[]{:T(128)}, f32[1,2,256]{2,1,0:T(2,128)S(1)}, ...), condition=%wide.region_6.7_spmd.clone, body=%wide.region_3.6_spmd.clone.sunk | while | flops 545459200 | bytes 31097480 | solution.py:116
  171.9 3.5 fusion.134
  178.9 3.5 fusion.134
  185.9 3.5 fusion.134
  192.9 3.5 fusion.134
  200.2 4.1 all-to-all-start
  205.4 13.6 %all-to-all-done = bf16[4,64,2048]{2,1,0:T(8,128)(2,1)S(1)} async-done(((bf16[4,64,2048]{2,1,0:T(8,128)(2,1)}), bf16[4,64,2048]{2,1,0:T(8,128)(2,1)S(1)}, u32[]{:S(2)}, u32[]{:S(2)}) %all-to-all-start) | async-done | bytes 1048608 | tf_op jit(solution)/shard_map/all_to_all | solution.py:31
  220.4 42.0 %all_to_all.30 = bf16[32,4,2048]{2,1,0:T(4,128)(2,1)} all-to-all(bf16[32,4,2048]{2,1,0:T(4,128)(2,1)S(1)} %get-tuple-element.245), channel_id=1, replica_groups=mesh['grp'=2,'sp'=32,'tp'=4] {'sp'}, dimensions={0} | all-to-all | bytes 1048576 | tf_op jit(solution)/shard_map/all_to_all | solution.py:48
  262.6 37.5 %all_to_all.31 = bf16[32,4,2048]{2,1,0:T(4,128)(2,1)} all-to-all(bf16[32,4,2048]{2,1,0:T(4,128)(2,1)S(1)} %get-tuple-element.246), channel_id=1, replica_groups=mesh['grp'=2,'sp'=32,'tp'=4] {'sp'}, dimensions={0} | all-to-all | bytes 1048576 | tf_op jit(solution)/shard_map/all_to_all | solution.py:48
  302.7 4.5 fusion.56
  309.9 5.7 %fusion.67 = bf16[4,1,32,4,2048]{4,2,3,1,0:T(8,128)(2,1)} fusion(bf16[1,896,2048]{2,1,0:T(8,128)(2,1)} %param.39, bf16[4,32,4,896]{3,2,1,0:T(4,128)(2,1)S(1)} %dot_general.55), kind=kOutput, calls=%fused_computation.67 | convolution fusion | flops 1880096768 | bytes 6684672 | tf_op jit(solution)/shard_map/dot_general | solution.py:224
  315.6 3.9 all-to-all-start.2
  319.5 11.3 %all-gather.8.cloned.1.call-done = bf16[128,4,2048]{2,1,0:T(4,128)(2,1)} async-done(((bf16[32,4,2048]{2,1,0:T(4,128)(2,1)}), bf16[128,4,2048]{2,1,0:T(4,128)(2,1)}) %all-gather.8.cloned.1.call-update) | async-done | bytes 2097168 | tf_op jit(solution)/shard_map/all_gather | solution.py:236
  330.8 4.0 reshape_reshape.7
  334.8 5.1 %fusion.54 = f32[512,896]{1,0:T(8,128)S(1)} fusion(bf16[512,2048]{1,0:T(8,128)(2,1)} %reshape_reshape.7, bf16[1,2048,896]{2,1,0:T(8,128)(2,1)} %param.37), kind=kOutput, calls=%fused_computation.60 | convolution fusion | flops 1879048192 | bytes 7602176 | tf_op jit(solution)/shard_map/dot_general | solution.py:221
  343.5 6.0 %fusion.64 = bf16[4,1,32,4,2048]{4,2,3,1,0:T(8,128)(2,1)} fusion(bf16[1,896,2048]{2,1,0:T(8,128)(2,1)} %param.39, bf16[4,32,4,896]{3,2,1,0:T(4,128)(2,1)} %dot_general.59), kind=kOutput, calls=%fused_computation.66 | convolution fusion | flops 1880096768 | bytes 6684672 | tf_op jit(solution)/shard_map/dot_general | solution.py:224
  349.9 4.5 all-to-all-start.4
  354.8 25.0 %all-to-all-done.4 = bf16[4,1,32,4,2048]{4,2,3,1,0:T(8,128)(2,1)} async-done(((bf16[4,1,32,4,2048]{4,2,3,1,0:T(8,128)(2,1)}), bf16[4,1,32,4,2048]{4,2,3,1,0:T(8,128)(2,1)}, u32[]{:S(2)}, u32[]{:S(2)}) %all-to-all-start.4) | async-done | bytes 2097184 | tf_op jit(solution)/shard_map/all_to_all | solution.py:31
  382.6 79.1 %all_to_all.32 = bf16[32,8,2048]{2,1,0:T(8,128)(2,1)S(1)} all-to-all(bf16[32,8,2048]{2,1,0:T(8,128)(2,1)S(1)} %copy.141), channel_id=1, replica_groups=mesh['grp'=2,'sp'=32,'tp'=4] {'sp'}, dimensions={0} | all-to-all | bytes 2097152 | tf_op jit(solution)/shard_map/all_to_all | solution.py:240
  (191 shorter events, 54.6 us)
Async XLA Ops:
  6.5 191.7 %copy-start = (bf16[256,2048]{1,0:T(8,128)(2,1)S(1)}, bf16[256,2048]{1,0:T(8,128)(2,1)}, u32[]{:S(2)}) copy-start(bf16[256,2048]{1,0:T(8,128)(2,1)} %param.34) | copy-start | bytes 3145732
  6.6 5.7 %copy-start.6 = (bf16[256,64]{0,1:T(8,128)(2,1)S(1)}, bf16[256,64]{0,1:T(8,128)(2,1)}, u32[]{:S(2)}) copy-start(bf16[256,64]{0,1:T(8,128)(2,1)} %param.28) | copy-start | bytes 98308
  6.6 5.8 %copy-start.16 = (f32[64]{0:T(128)S(1)}, f32[64]{0:T(128)}, u32[]{:S(2)}) copy-start(f32[64]{0:T(128)} %param.33) | copy-start | bytes 772
  6.6 5.9 %copy-start.13 = (bf16[256,64]{0,1:T(8,128)(2,1)S(1)}, bf16[256,64]{0,1:T(8,128)(2,1)}, u32[]{:S(2)}) copy-start(bf16[256,64]{0,1:T(8,128)(2,1)} %param.29) | copy-start | bytes 98308
  6.6 6.7 %copy-start.12 = (bf16[256,128]{1,0:T(8,128)(2,1)S(1)}, bf16[256,128]{1,0:T(8,128)(2,1)}, u32[]{:S(2)}) copy-start(bf16[256,128]{1,0:T(8,128)(2,1)} %param.27) | copy-start | bytes 196612
  6.6 6.9 %copy-start.18 = (f32[64]{0:T(128)S(1)}, f32[64]{0:T(128)}, u32[]{:S(2)}) copy-start(f32[64]{0:T(128)} %param.32) | copy-start | bytes 772
  6.6 7.0 %copy-start.8 = (bf16[256,256]{1,0:T(8,128)(2,1)S(1)}, bf16[256,256]{1,0:T(8,128)(2,1)}, u32[]{:S(2)}) copy-start(bf16[256,256]{1,0:T(8,128)(2,1)} %param.24) | copy-start | bytes 393220
  6.6 7.1 %copy-start.17 = (f32[128]{0:T(128)S(1)}, f32[128]{0:T(128)}, u32[]{:S(2)}) copy-start(f32[128]{0:T(128)} %param.30) | copy-start | bytes 1540
  6.6 107.2 %all-gather.4.cloned.1.call-start = ((), (), s32[]{:S(2)}) async-start(), calls=%async_computation.6 | async-start | bytes 6488064 | tf_op jit(solution)/shard_map/all_gather | solution.py:16
  126.0 3.8 copy-start.2
  134.7 3.8 copy-start.2
  143.4 3.8 copy-start.2
  152.1 3.8 copy-start.2
  169.2 28.1 %copy-start.11 = (f32[1,2,256]{2,1,0:T(2,128)S(1)}, f32[1,2,256]{2,1,0:T(2,128)}, u32[]{:S(2)}) copy-start(f32[1,2,256]{2,1,0:T(2,128)} %get-tuple-element.84) | copy-start | bytes 6148
  171.9 3.6 copy-start.3
  178.9 3.6 copy-start.3
  185.9 3.6 copy-start.3
  192.9 3.6 copy-start.3
  197.3 1.5 copy-start.5
  198.8 5.6 %copy-start.15 = (s32[64,2]{0,1:T(2,128)S(1)}, s32[64,2]{0,1:T(2,128)}, u32[]{:S(2)}) copy-start(s32[64,2]{0,1:T(2,128)} %param.40) | copy-start | bytes 1540
  200.2 18.9 %copy-start.7 = (bf16[64,2048]{1,0:T(8,128)(2,1)S(1)}, bf16[64,2048]{1,0:T(8,128)(2,1)}, u32[]{:S(2)}) copy-start(bf16[64,2048]{1,0:T(8,128)(2,1)} %param.23) | copy-start | bytes 786436
  200.2 19.1 %copy-start.14 = (f32[2048]{0:T(1024)S(1)}, f32[2048]{0:T(1024)}, u32[]{:S(2)}) copy-start(f32[2048]{0:T(1024)} %param.36) | copy-start | bytes 24580
  200.2 18.8 %all-to-all-start = ((bf16[4,64,2048]{2,1,0:T(8,128)(2,1)}), bf16[4,64,2048]{2,1,0:T(8,128)(2,1)S(1)}, u32[]{:S(2)}, u32[]{:S(2)}) async-start(bf16[4,64,2048]{2,1,0:T(8,128)(2,1)} %bitcast.20), calls=%async_computation | async-start | bytes 2097152 | tf_op jit(solution)/shard_map/all_to_all | solution.py:31
  204.3 95.8 %all-gather.6.cloned.1.call-start = ((), (), s32[]{:S(2)}) async-start(), calls=%async_computation.7 | async-start | bytes 2621440 | tf_op jit(solution)/shard_map/all_gather | solution.py:236
  262.5 68.3 %all-gather.8.cloned.1.call-start = ((), (), s32[]{:S(2)}) async-start(), calls=%async_computation.8 | async-start | bytes 2621440 | tf_op jit(solution)/shard_map/all_gather | solution.py:236
  302.7 4.5 copy-start.20
  315.6 34.3 %all-to-all-start.2 = ((bf16[4,1,32,4,2048]{4,2,3,1,0:T(8,128)(2,1)}), bf16[4,1,32,4,2048]{4,2,3,1,0:T(8,128)(2,1)S(1)}, u32[]{:S(2)}, u32[]{:S(2)}) async-start(bf16[4,1,32,4,2048]{4,2,3,1,0:T(8,128)(2,1)} %fusion.67), calls=%async_computation.2 | async-start | bytes 4194304 | tf_op jit(solution)/shard_map/all_to_all | solution.py:31
  334.8 5.2 %copy-start.4 = (bf16[512,2048]{1,0:T(8,128)(2,1)S(1)}, bf16[512,2048]{1,0:T(8,128)(2,1)}, u32[]{:S(2)}) copy-start(bf16[512,2048]{1,0:T(8,128)(2,1)} %reshape_reshape.7) | copy-start | bytes 6291460
  334.8 5.2 %copy-start.21 = (bf16[1,2048,896]{2,1,0:T(8,128)(2,1)S(1)}, bf16[1,2048,896]{2,1,0:T(8,128)(2,1)}, u32[]{:S(2)}) copy-start(bf16[1,2048,896]{2,1,0:T(8,128)(2,1)} %param.38) | copy-start | bytes 11010052
  349.9 29.9 %all-to-all-start.4 = ((bf16[4,1,32,4,2048]{4,2,3,1,0:T(8,128)(2,1)}), bf16[4,1,32,4,2048]{4,2,3,1,0:T(8,128)(2,1)}, u32[]{:S(2)}, u32[]{:S(2)}) async-start(bf16[4,1,32,4,2048]{4,2,3,1,0:T(8,128)(2,1)} %fusion.64), calls=%async_computation.4 | async-start | bytes 4194304 | tf_op jit(solution)/shard_map/all_to_all | solution.py:31
  382.0 79.7 %copy-start.19 = (f32[64,2]{0,1:T(2,128)S(1)}, f32[64,2]{0,1:T(2,128)}, u32[]{:S(2)}) copy-start(f32[64,2]{0,1:T(2,128)} %param.41) | copy-start | bytes 1540
  382.0 80.8 %copy-start.1 = (bf16[256,2048]{1,0:T(8,128)(2,1)S(1)}, bf16[256,2048]{1,0:T(8,128)(2,1)}, u32[]{:S(2)}) copy-start(bf16[256,2048]{1,0:T(8,128)(2,1)} %param.34) | copy-start | bytes 3145732
  (8 other events, 5.0 us)
Sparse Core Ops, SparseCore 0:
  13.4 100.3 all-gather.3
  262.6 26.0 all-gather.5
  300.2 30.5 all-gather.7
where the time goes:
time: 471 us; the launch traced here: 469 us
  blocking collectives  159 us (34%)
  waiting for transfers between devices  149 us (32%)
  matrix products  83 us (18%)
  local copies, waits for them, and re-layouts  35.1 us (7%)
  other arithmetic  16.5 us (4%)
  between operations  13.7 us (3%)
  starting transfers between devices  12.7 us (3%)
    all_gather x1, waiting for transfers between devices, sent_together(): lax.all_gather(both, axis, axis=dim, tiled=True)  98.7 us
    all_to_all x2, blocking collectives, items_in_groups(): lax.all_to_all(group, axis, split_axis=split_dim, concat_axis=concat_dim,...  79.5 us
    all_to_all x1, blocking collectives, body(): lax.all_to_all(results, 'sp', split_axis=0, concat_axis=0, tiled=True)  79.1 us
    all_to_all x3, waiting for transfers between devices, sum_at_owner(): lax.all_to_all(in_blocks(value, dim, peers), axis, 0, 0, tiled=True)  39.1 us
    dot_general x8, matrix products, step(): jnp.einsum('hgqk,khd->qhgd', weights.astype(jnp.bfloat16), value_block, p...  29.2 us
    dot_general x8, matrix products, step(): jnp.einsum('qhgd,khd->hgqk', queries, key_block, preferred_element_type=j...  25 us
    all_to_all x3, starting transfers between devices, sum_at_owner(): lax.all_to_all(in_blocks(value, dim, peers), axis, 0, 0, tiled=True)  12.6 us
    dot_general x2, matrix products, expert_block(): jnp.dot(hidden, down_weight[0], preferred_element_type=jnp.float32)  11.7 us
  transfers between devices with their start and end apart: 6, of which 5 were waited for; matrix products, arithmetic and copies ran while one was open for 8% of the time, Pallas kernels for 0%

commit v1 on v0

v1 whole, which is shorter than its diff:
```python
import functools
import math

import jax
import jax.numpy as jnp
from jax import lax
from jax.experimental import pallas as pl
from jax.experimental.pallas import tpu as pltpu
from jax.sharding import PartitionSpec as P

GRID = 64
THETA = 10000.0
EPS = 1e-06
NEG_BIG = -1e30
LOG2E = math.log2(math.e)
MESH = pl.DeviceIdType.MESH
F32 = jnp.float32
BF16 = jnp.bfloat16


def in_blocks(value, dim, peers):
    lengths = value.shape
    blocks = value.reshape(*lengths[:dim], peers, lengths[dim] // peers, *lengths[dim + 1 :])
    return jnp.moveaxis(blocks, dim, 0)


def sum_at_owner(value, axis, dim):
    peers = lax.axis_size(axis)
    blocks = lax.all_to_all(in_blocks(value, dim, peers), axis, 0, 0, tiled=True)
    return jnp.sum(blocks.astype(jnp.float32), axis=0)


def items_in_groups(value, axis, split_dim, concat_dim, work, item_dim, out_dim):
    items = jax.tree.leaves(value)[0].shape[item_dim]
    count = 2 if items % 2 == 0 else 1
    finished = []
    for k in range(count):
        group = jax.tree.map(
            lambda a: lax.slice_in_dim(
                a, k * (items // count), (k + 1) * (items // count), axis=item_dim
            ),
            value,
        )
        finished.append(
            work(
                lax.all_to_all(
                    group, axis, split_axis=split_dim, concat_axis=concat_dim, tiled=True
                )
            )
        )
    return jax.tree.map(lambda *parts: jnp.concatenate(parts, axis=out_dim), *finished)


def angles_of(places, head_width):
    quarter = head_width // 4
    inv_freq = THETA ** (-jnp.arange(quarter, dtype=jnp.float32) / quarter)
    grid_rows = (places // GRID).astype(jnp.float32)
    grid_cols = (places % GRID).astype(jnp.float32)
    row_angle = grid_rows[:, None] * inv_freq[None, :]
    col_angle = grid_cols[:, None] * inv_freq[None, :]
    return jnp.concatenate([row_angle, row_angle, col_angle, col_angle], axis=-1)


def lane_ids(shape):
    return lax.broadcasted_iota(jnp.int32, shape, 1)


def turned_lanes(values, quarter):
    lanes = lane_ids(values.shape)
    width = values.shape[1]
    return jnp.where(
        lanes % (2 * quarter) < quarter,
        pltpu.roll(values, width - quarter, 1),
        pltpu.roll(values, quarter, 1),
    )


def rotate(values, cos_table, sin_table, quarter):
    return values * cos_table + turned_lanes(values, quarter) * sin_table


def norm_wide(values, gain):
    mean = jnp.mean(values * values, axis=-1, keepdims=True)
    return values * lax.rsqrt(mean + EPS) * gain


def norm_halves(values, gain):
    lanes = lane_ids(values.shape)
    half = values.shape[1] // 2
    squares = values * values
    low = jnp.sum(jnp.where(lanes < half, squares, 0.0), axis=-1, keepdims=True) / half
    high = jnp.sum(jnp.where(lanes < half, 0.0, squares), axis=-1, keepdims=True) / half
    scale = jnp.where(lanes < half, lax.rsqrt(low + EPS), lax.rsqrt(high + EPS))
    return values * scale * gain


def attend_kernel(
    chips,
    peers,
    qw_ref,
    kw_ref,
    vw_ref,
    qn_ref,
    kvn_ref,
    gains_ref,
    tables_ref,
    res_ref,
    norm_gain_ref,
    ow_hbm,
    on_hbm,
    att_ref,
    normed_ref,
    kv_buf,
    qws,
    qns,
    m_buf,
    l_buf,
    acc_buf,
    heads,
    ow_buf,
    on_buf,
    part,
    first_in,
    last_in,
    w_sem,
    zsend,
    zrecv,
    psend,
    precv,
    xsend,
    xrecv,
):
    tok = qw_ref.shape[0]
    half = tok // 2
    wide = kw_ref.shape[1]
    sp = lax.axis_index("sp")
    tp = lax.axis_index("tp")
    z, core = sp // 2, sp % 2
    far = chips // 2
    right = {"sp": ((z + 1) % chips) * 2 + core}
    left = {"sp": ((z + chips - 1) % chips) * 2 + core}
    mate = {"sp": z * 2 + (1 - core)}
    xright = {"tp": (tp + 1) % peers}
    xleft = {"tp": (tp + peers - 1) % peers}

    w_copies = [
        pltpu.make_async_copy(ow_hbm, ow_buf, w_sem.at[0]),
        pltpu.make_async_copy(on_hbm, on_buf, w_sem.at[1]),
    ]
    for copy in w_copies:
        copy.start()

    barrier = pltpu.get_barrier_semaphore()
    for other in (right, left, mate, xright, xleft):
        pl.semaphore_signal(barrier, inc=1, device_id=other, device_id_type=MESH)

    def rows_of(chip, owner, sub):
        at = pl.multiple_of((chip * 2 + owner) * tok + sub * half, half)
        return kv_buf.at[pl.ds(at, half)]

    cos_w, sin_w = tables_ref[0], tables_ref[1]
    cos_n, sin_n = tables_ref[2], tables_ref[3]
    own = pl.ds(pl.multiple_of(sp * tok, tok), tok)
    k_wide = rotate(norm_wide(kw_ref[...].astype(F32), gains_ref[1:2]), cos_w, sin_w, wide // 4)
    kvn = kvn_ref[...].astype(F32)
    k_narrow = rotate(norm_halves(kvn, gains_ref[3:4]), cos_n, sin_n, wide // 8)
    kv_buf[own, 0:wide] = k_wide.astype(BF16)
    kv_buf[own, wide : 2 * wide] = vw_ref[...]
    kv_buf[own, 2 * wide : 3 * wide] = jnp.where(
        lane_ids(kvn.shape) < wide // 2, k_narrow, kvn
    ).astype(BF16)

    pl.semaphore_wait(barrier, 5)

    def z_copy(way, step, sub):
        shift = step - 1
        chip = (z + chips - shift) % chips if way == 0 else (z + shift) % chips
        ref = rows_of(chip, core, sub)
        return pltpu.make_async_remote_copy(
            src_ref=ref,
            dst_ref=ref,
            send_sem=zsend.at[way, step - 1, sub],
            recv_sem=zrecv.at[way, step - 1, sub],
            device_id=right if way == 0 else left,
            device_id_type=MESH,
        )

    def z_arrival(way, step, sub):
        chip = (z + chips - step) % chips if way == 0 else (z + step) % chips
        ref = rows_of(chip, core, sub)
        return pltpu.make_async_remote_copy(
            src_ref=ref,
            dst_ref=ref,
            send_sem=zsend.at[way, step - 1, sub],
            recv_sem=zrecv.at[way, step - 1, sub],
            device_id=right if way == 0 else left,
            device_id_type=MESH,
        )

    def m_copy(way, step, sub, owner):
        chip = (z + chips - step) % chips if way == 0 else (z + step) % chips
        ref = rows_of(chip, owner, sub)
        return pltpu.make_async_remote_copy(
            src_ref=ref,
            dst_ref=ref,
            send_sem=psend.at[way, step, sub],
            recv_sem=precv.at[way, step, sub],
            device_id=mate,
            device_id_type=MESH,
        )

    for way, sub in ((0, 0), (1, 1), (0, 1), (1, 0)):
        z_copy(way, 1, sub).start()
    for sub in (0, 1):
        m_copy(0, 0, sub, core).start()

    qw = qw_ref[...].astype(F32)
    for head in (0, 1):
        q = norm_wide(qw[:, head * wide : (head + 1) * wide], gains_ref[0:1])
        qws[head * tok : (head + 1) * tok] = rotate(q, cos_w, sin_w, wide // 4).astype(BF16)
    qn = rotate(norm_halves(qn_ref[...].astype(F32), gains_ref[2:3]), cos_n, sin_n, wide // 8)
    low = lane_ids(qn.shape) < wide // 2
    qns[0:tok] = jnp.where(low, qn, 0.0).astype(BF16)
    qns[tok : 2 * tok] = jnp.where(low, pltpu.roll(qn, wide // 2, 1), 0.0).astype(BF16)
    m_buf[...] = jnp.full(m_buf.shape, NEG_BIG, F32)
    l_buf[...] = jnp.zeros(l_buf.shape, F32)
    acc_buf[...] = jnp.zeros(acc_buf.shape, F32)

    def attend_chip(chip):
        keys = pl.ds(pl.multiple_of(chip * 2 * tok, 2 * tok), 2 * tok)
        k_w, v_w = kv_buf[keys, 0:wide], kv_buf[keys, wide : 2 * wide]
        kv_n = kv_buf[keys, 2 * wide : 3 * wide]
        work = []
        for kind in (0, 1):
            for head in (0, 1):
                work.append((kind, head))

        def scores(kind, head):
            q = (qws if kind == 0 else qns)[head * tok : (head + 1) * tok]
            return lax.dot_general(
                q,
                k_w if kind == 0 else kv_n,
                (((1,), (1,)), ((), ())),
                preferred_element_type=F32,
            )

        upcoming = scores(*work[0])
        for at, (kind, head) in enumerate(work):
            s = upcoming
            if at + 1 < len(work):
                upcoming = scores(*work[at + 1])
            factor = LOG2E * (wide if kind == 0 else wide // 2) ** (-0.5)
            m_old = m_buf[at]
            m_new = jnp.maximum(m_old, jnp.max(s, axis=-1, keepdims=True))
            alpha = jnp.exp2((m_old - m_new) * factor)
            parts = [
                jnp.exp2((s[:, i * wide : (i + 1) * wide] - m_new) * factor)
                for i in range(s.shape[1] // wide)
            ]
            total = parts[0]
            for p in parts[1:]:
                total = total + p
            weights = jnp.concatenate([p.astype(BF16) for p in parts], axis=1)
            mixed = jnp.dot(
                weights, v_w if kind == 0 else kv_n, preferred_element_type=F32
            )
            m_buf[at] = m_new
            l_buf[at] = l_buf[at] * alpha + total
            acc_buf[at] = acc_buf[at] * alpha + mixed

    def ring_step(step, nothing):
        @pl.when(step <= far)
        def _():
            for turn in (0, 1):
                for way in (0, 1):
                    sub = turn if way == 0 else 1 - turn

                    def arrived(way=way, sub=sub, turn=turn):
                        z_arrival(way, step, sub).wait_recv()
                        if turn == 0:

                            @pl.when(step < far)
                            def _():
                                z_copy(way, step + 1, sub).start()
                        else:

                            @pl.when(step < far - 1)
                            def _():
                                z_copy(way, step + 1, sub).start()

                        m_copy(way, step, sub, core).start()

                    if turn == 0:
                        arrived()
                    else:
                        pl.when(step < far)(arrived)

        before = step - 1

        @pl.when(before == 0)
        def _():
            for sub in (0, 1):
                m_copy(0, 0, sub, 1 - core).wait_recv()

        @pl.when(before > 0)
        def _():
            m_copy(0, before, 0, 1 - core).wait_recv()
            m_copy(1, before, 1, 1 - core).wait_recv()

        @pl.when(jnp.logical_and(before > 0, before < far))
        def _():
            m_copy(0, before, 1, 1 - core).wait_recv()
            m_copy(1, before, 0, 1 - core).wait_recv()

        def one(side, nothing):
            attend_chip((z + chips + before * (2 * side - 1)) % chips)
            return nothing

        single = jnp.logical_or(before == 0, before == far)
        return lax.fori_loop(0, jnp.where(single, 1, 2), one, nothing)

    lax.fori_loop(1, far + 2, ring_step, 0)

    outs = []
    for at in range(4):
        outs.append(acc_buf[at] / jnp.sum(l_buf[at], axis=-1, keepdims=True))
    heads[:, 0:wide] = outs[0].astype(BF16)
    heads[:, wide : 2 * wide] = outs[1].astype(BF16)
    heads[:, 2 * wide : 3 * wide] = jnp.where(
        low, pltpu.roll(outs[2], wide // 2, 1), outs[3]
    ).astype(BF16)
    for copy in w_copies:
        copy.wait()

    rows = res_ref.shape[0]
    cols = res_ref.shape[1] // 2

    def x_copy(way, number):
        dest = (tp + 1) % peers if way == 0 else (tp + peers - 1) % peers
        with_far = way * cols
        alone = (1 - way) * cols
        if number == 0:
            src = part.at[(tp + 2) % peers, :, pl.ds(with_far, cols)]
            dst = first_in.at[way]
        else:
            at = pl.ds(alone if number == 1 else with_far, cols)
            src = part.at[dest, :, at]
            dst = last_in.at[way, :, at]
        return pltpu.make_async_remote_copy(
            src_ref=src,
            dst_ref=dst,
            send_sem=xsend.at[way, number],
            recv_sem=xrecv.at[way, number],
            device_id=xright if way == 0 else xleft,
            device_id_type=MESH,
        )

    def project(peer):
        h = heads[pl.ds(pl.multiple_of(peer * rows, rows), rows)]
        product = jnp.dot(h[:, 0 : 2 * wide], ow_buf[...], preferred_element_type=F32)
        product = product + jnp.dot(
            h[:, 2 * wide : 3 * wide], on_buf[...], preferred_element_type=F32
        )
        part[peer] = product.astype(BF16)

    project((tp + 2) % peers)
    x_copy(0, 0).start()
    x_copy(1, 0).start()
    project((tp + 1) % peers)
    x_copy(0, 1).start()
    project((tp + peers - 1) % peers)
    x_copy(1, 1).start()
    project(tp)
    for way in (0, 1):
        dest = (tp + 1) % peers if way == 0 else (tp + peers - 1) % peers
        x_copy(way, 0).wait_recv()
        at = slice(way * cols, (way + 1) * cols)
        part[dest, :, at] = (
            part[dest, :, at].astype(F32) + first_in[way].astype(F32)
        ).astype(BF16)
        x_copy(way, 2).start()
    for way in (0, 1):
        x_copy(way, 1).wait_recv()
        x_copy(way, 2).wait_recv()
    total = res_ref[...].astype(F32) + part[tp].astype(F32)
    total = total + last_in[0].astype(F32) + last_in[1].astype(F32)
    attended = total.astype(BF16)
    att_ref[...] = attended
    state = attended.astype(F32)
    mean = jnp.mean(state * state, axis=-1, keepdims=True)
    normed_ref[...] = (state * lax.rsqrt(mean + EPS) * norm_gain_ref[...]).astype(BF16)

    for way in (0, 1):
        for number in (0, 1, 2):
            x_copy(way, number).wait_send()
    for sub in (0, 1):
        m_copy(0, 0, sub, core).wait_send()

    def drain(step, nothing):
        for way in (0, 1):
            for sub in (0, 1):
                z_copy(way, step, sub).wait_send()
                m_copy(way, step, sub, core).wait_send()
        return nothing

    lax.fori_loop(1, far, drain, 0)
    for way in (0, 1):
        z_copy(way, far, way).wait_send()
        m_copy(way, far, way, core).wait_send()


def attend(
    residual,
    queries_wide,
    keys_wide,
    values_wide,
    queries_narrow,
    keys_narrow,
    values_narrow,
    gains,
    tables,
    norm_gain,
    output_wide,
    output_narrow,
):
    chips = lax.axis_size("sp") // 2
    peers = lax.axis_size("tp")
    tok, wide = keys_wide.shape
    rows, width = residual.shape
    far = chips // 2
    vmem = pl.BlockSpec(memory_space=pltpu.VMEM)
    hbm = pl.BlockSpec(memory_space=pl.ANY)
    dma = pltpu.SemaphoreType.DMA
    return pl.pallas_call(
        functools.partial(attend_kernel, chips, peers),
        out_shape=(
            jax.ShapeDtypeStruct((rows, width), BF16),
            jax.ShapeDtypeStruct((rows, width), BF16),
        ),
        in_specs=[vmem] * 9 + [hbm] * 2,
        out_specs=(vmem, vmem),
        scratch_shapes=[
            pltpu.VMEM((2 * chips * tok, 3 * wide), BF16),
            pltpu.VMEM((2 * tok, wide), BF16),
            pltpu.VMEM((2 * tok, wide), BF16),
            pltpu.VMEM((4, tok, wide), F32),
            pltpu.VMEM((4, tok, wide), F32),
            pltpu.VMEM((4, tok, wide), F32),
            pltpu.VMEM((tok, 3 * wide), BF16),
            pltpu.VMEM(output_wide.shape, BF16),
            pltpu.VMEM(output_narrow.shape, BF16),
            pltpu.VMEM((peers, rows, width), BF16),
            pltpu.VMEM((2, rows, width // 2), BF16),
            pltpu.VMEM((2, rows, width), BF16),
            dma((2,)),
            dma((2, far, 2)),
            dma((2, far, 2)),
            dma((2, far + 1, 2)),
            dma((2, far + 1, 2)),
            dma((2, 3)),
            dma((2, 3)),
        ],
        compiler_params=pltpu.CompilerParams(
            collective_id=0, has_side_effects=True, vmem_limit_bytes=40 * 1024 * 1024
        ),
        name="attend",
    )(
        queries_wide,
        keys_wide,
        values_wide,
        queries_narrow,
        jnp.concatenate([keys_narrow, values_narrow], axis=1),
        gains,
        tables,
        residual,
        norm_gain.reshape(1, width),
        output_wide,
        output_narrow,
    )


def slot_tables(chosen, slot_count, expert_count):
    row_count = chosen.shape[0]
    pick_count = chosen.shape[1]
    flat_pick = chosen.reshape(row_count * pick_count)
    hit_marks = (flat_pick[:, None] == jnp.arange(expert_count, dtype=jnp.int32)[None, :]).astype(
        jnp.int32
    )
    before = jnp.cumsum(hit_marks, axis=0) - hit_marks
    slot_place = jnp.sum(before * hit_marks, axis=1)
    target = flat_pick * slot_count + slot_place
    slot_table = target[:, None] == jnp.arange(expert_count * slot_count, dtype=jnp.int32)[None, :]
    return slot_table.astype(jnp.bfloat16).reshape(row_count, pick_count, expert_count * slot_count)


def body(
    residual,
    queries_wide,
    keys_wide,
    values_wide,
    queries_narrow,
    keys_narrow,
    values_narrow,
    query_gain_wide,
    key_gain_wide,
    query_gain_narrow,
    key_gain_narrow,
    output_wide,
    output_narrow,
    norm_gain,
    gate_weight,
    up_weight,
    down_weight,
    route_ids,
    route_weights,
):
    tok_count = queries_wide.shape[0]
    places = lax.axis_index("sp") * tok_count + jnp.arange(tok_count, dtype=jnp.int32)
    wide_width = query_gain_wide.shape[0]
    narrow_width = query_gain_narrow.shape[0]
    wide_angles = angles_of(places, wide_width)
    narrow_angles = angles_of(places, narrow_width)
    narrow_angles = jnp.concatenate([narrow_angles, narrow_angles], axis=1)
    lanes = jnp.arange(wide_width, dtype=jnp.int32)
    wide_sign = jnp.where(lanes % (wide_width // 2) < wide_width // 4, -1.0, 1.0)
    narrow_sign = jnp.where(lanes % (narrow_width // 2) < narrow_width // 4, -1.0, 1.0)
    tables = jnp.stack(
        [
            jnp.cos(wide_angles),
            jnp.sin(wide_angles) * wide_sign,
            jnp.cos(narrow_angles),
            jnp.sin(narrow_angles) * narrow_sign,
        ]
    )
    gains = jnp.stack(
        [
            query_gain_wide,
            key_gain_wide,
            jnp.concatenate([query_gain_narrow, query_gain_narrow]),
            jnp.concatenate([key_gain_narrow, key_gain_narrow]),
        ]
    )
    attended, normed = attend(
        residual,
        queries_wide,
        keys_wide,
        values_wide,
        queries_narrow,
        keys_narrow,
        values_narrow,
        gains,
        tables,
        norm_gain,
        output_wide,
        output_narrow,
    )
    own_rows = residual.shape[0]
    state_float = attended.astype(jnp.float32)
    pick_count = route_ids.shape[1]
    expert_count = lax.axis_size("sp")
    slot_count = 2 * pick_count * own_rows // expert_count
    model_width = residual.shape[1]
    own_tables = slot_tables(route_ids, slot_count, expert_count)

    def expert_block(arrived):
        full_shape = arrived.shape
        flat_rows = arrived.reshape(-1, model_width)
        gate_act = jnp.dot(flat_rows, gate_weight[0], preferred_element_type=jnp.float32)
        up_act = jnp.dot(flat_rows, up_weight[0], preferred_element_type=jnp.float32)
        hidden = (jax.nn.silu(gate_act) * up_act).astype(jnp.bfloat16)
        partial_value = jnp.dot(hidden, down_weight[0], preferred_element_type=jnp.float32).reshape(
            full_shape
        )
        summed = sum_at_owner(partial_value.astype(jnp.bfloat16), "tp", 0)
        return summed.reshape(full_shape[1:]).astype(jnp.bfloat16)

    send_rows = jnp.einsum(
        "rks,rd->sd", own_tables, normed, preferred_element_type=jnp.float32
    ).astype(jnp.bfloat16)
    send_rows = send_rows.reshape(expert_count, slot_count, model_width)

    def copy_then_run(arrived):
        copies = lax.all_gather(arrived, "tp", axis=0, tiled=True)
        return expert_block(copies.reshape((lax.axis_size("tp"),) + arrived.shape))

    results = items_in_groups(send_rows, "sp", 0, 0, copy_then_run, 1, 1)
    returned = lax.all_to_all(results, "sp", split_axis=0, concat_axis=0, tiled=True)
    returned_flat = returned.reshape(expert_count * slot_count, model_width)
    picked = jnp.einsum(
        "rks,sd->rkd", own_tables, returned_flat, preferred_element_type=jnp.float32
    )
    mixture = jnp.sum(route_weights[:, :, None] * picked, axis=1)
    return (state_float + mixture).astype(jnp.bfloat16)


def solution(mesh):
    return jax.shard_map(
        body,
        mesh=mesh,
        in_specs=(
            P(("grp", "sp", "tp"), None),
            P(("grp", "sp"), "tp"),
            P(("grp", "sp"), "tp"),
            P(("grp", "sp"), "tp"),
            P(("grp", "sp"), "tp"),
            P(("grp", "sp"), "tp"),
            P(("grp", "sp"), "tp"),
            P(),
            P(),
            P(),
            P(),
            P("tp", None),
            P("tp", None),
            P(),
            P("sp", None, "tp"),
            P("sp", None, "tp"),
            P("sp", "tp", None),
            P(("grp", "sp", "tp"), None),
            P(("grp", "sp", "tp"), None),
        ),
        out_specs=P(("grp", "sp", "tp"), None),
        check_vma=False,
    )
```

time: 471 us -> 337 us (0.72)
  waiting for transfers between devices: 149 us -> 39.5 us
  Pallas kernels: 0 us -> 76.6 us
  matrix products: 83 us -> 26.1 us
  local copies, waits for them, and re-layouts: 35.1 us -> 9.82 us
  other arithmetic: 16.5 us -> 7.59 us
  blocking collectives: 159 us -> 153 us
    all_gather x1 -> x0, waiting for transfers between devices: 98.7 us -> none  [sent_together(): lax.all_gather(both, axis, axis=dim, tiled=True)]
    pallas_call x0 -> x1, Pallas kernels: none -> 76.6 us  [attend(): pl.pallas_call(functools.partial(attend_kernel, chips, peers), out_shape=...]
    dot_general x18 -> x0, matrix products: 56 us -> none  [the longest x8 29.2 us: step(): jnp.einsum('hgqk,khd->qhgd', weights.astype(jnp.bfloat16), value_block, p...]
    all_to_all x3 -> x2, waiting for transfers between devices: 39.1 us -> 26.6 us  [sum_at_owner(): lax.all_to_all(in_blocks(value, dim, peers), axis, 0, 0, tiled=True)]
    slice x3 -> x0, local copies, waits for them, and re-layouts: 11.5 us -> none  [sent_together(): finished.append(lax.slice_in_dim(out, at, at + a.shape[along], axis=along))]
    reduce_sum x13 -> x0, other arithmetic: 6.67 us -> none  [the longest x8 5.59 us: step(): weight_sum = weight_sum * rescale + jnp.sum(weights, axis=-1)]
    unnamed x45 -> x33, local copies, waits for them, and re-layouts: 8.1 us -> 2.73 us
    all_to_all x3 -> x2, starting transfers between devices: 12.6 us -> 9.28 us  [sum_at_owner(): lax.all_to_all(in_blocks(value, dim, peers), axis, 0, 0, tiled=True)]
  transfers between devices with their start and end apart: 6 -> 4, of which waited for: 5 -> 3; matrix products, arithmetic and copies ran while one was open for 8% -> 10% of each run, Pallas kernels for 0% -> 0%
where the time goes in v1:
time: 337 us; the launch traced here: 336 us
  blocking collectives  153 us (45%)
  Pallas kernels  76.6 us (23%)
  waiting for transfers between devices  39.5 us (12%)
  matrix products  26.1 us (8%)
  between operations  13.9 us (4%)
  local copies, waits for them, and re-layouts  9.82 us (3%)
  starting transfers between devices  9.34 us (3%)
  other arithmetic  7.59 us (2%)
    all_to_all x2, blocking collectives, items_in_groups(): lax.all_to_all(group, axis, split_axis=split_dim, concat_axis=concat_dim,...  77.3 us
    pallas_call x1, Pallas kernels, attend(): pl.pallas_call(functools.partial(attend_kernel, chips, peers), out_shape=...  76.6 us
    all_to_all x1, blocking collectives, body(): lax.all_to_all(results, 'sp', split_axis=0, concat_axis=0, tiled=True)  75.8 us
    all_to_all x2, waiting for transfers between devices, sum_at_owner(): lax.all_to_all(in_blocks(value, dim, peers), axis, 0, 0, tiled=True)  26.6 us
    all_gather x2, waiting for transfers between devices, copy_then_run(): copies = lax.all_gather(arrived, 'tp', axis=0, tiled=True)  12.9 us
    dot_general x2, matrix products, expert_block(): jnp.dot(hidden, down_weight[0], preferred_element_type=jnp.float32)  11.4 us
    all_to_all x2, starting transfers between devices, sum_at_owner(): lax.all_to_all(in_blocks(value, dim, peers), axis, 0, 0, tiled=True)  9.28 us
    dot_general x2, matrix products, expert_block(): jnp.dot(flat_rows, gate_weight[0], preferred_element_type=jnp.float32)  9.06 us
  transfers between devices with their start and end apart: 4, of which 3 were waited for; matrix products, arithmetic and copies ran while one was open for 10% of the time, Pallas kernels for 0%

profile of v1, /device:TPU:33, one launch (start us, length us, event | category | flops | bytes accessed | tf_op | source)
XLA Modules:
  0.0 336.0 jit_solution(11296296360624596914)
XLA Ops:
  7.0 1.0 copy.76
  8.0 0.9 copy.77
  8.9 0.8 copy.78
  10.5 0.7 multiply_add_fusion
  11.3 0.3 concatenate.64
  11.6 0.5 fusion.43
  12.3 0.6 fusion.38
  13.0 76.6 %attend.1 = (bf16[64,2048]{1,0:T(8,128)(2,1)S(1)}, bf16[64,2048]{1,0:T(8,128)(2,1)S(1)}) custom-call(bf16[256,256]{1,0:T(8,128)(2,1)S(1)} %copy-done.3, bf16[256,128]{1,0:T(8,128)(2,1)S(1)} %copy-done.4, bf16[256,128]{1,0:T(8,128)(2,1)S(1)} %copy-done.5, bf16[256,128]{1,0:T(8,128)(2,1)S(1)} %copy-done.6, bf16[256,128]{1,0:T(8,128)(2,1)S(1)} %pad_maximum_fusion.3.kvn_ref, ...), custom_call_target="tpu_custom_call" | custom-call | tf_op jit(solution)/shard_map/attend/pallas_call | solution.py:434
  89.6 0.5 fusion.24
  90.1 0.4 fusion.42
  90.4 39.8 %all_to_all.25 = bf16[32,4,2048]{2,1,0:T(4,128)(2,1)} all-to-all(bf16[32,4,2048]{2,1,0:T(4,128)(2,1)S(1)} %get-tuple-element.9), channel_id=1, replica_groups=mesh['grp'=2,'sp'=32,'tp'=4] {'sp'}, dimensions={0} | all-to-all | bytes 1048576 | tf_op jit(solution)/shard_map/all_to_all | solution.py:46
  130.4 37.5 %all_to_all.26 = bf16[32,4,2048]{2,1,0:T(4,128)(2,1)} all-to-all(bf16[32,4,2048]{2,1,0:T(4,128)(2,1)S(1)} %get-tuple-element.10), channel_id=1, replica_groups=mesh['grp'=2,'sp'=32,'tp'=4] {'sp'}, dimensions={0} | all-to-all | bytes 1048576 | tf_op jit(solution)/shard_map/all_to_all | solution.py:46
  167.9 2.5 reshape_reshape.6
  170.5 4.5 %fusion.10 = f32[512,896]{1,0:T(8,128)S(1)} fusion(bf16[512,2048]{1,0:T(8,128)(2,1)S(1)} %reshape_reshape.6, bf16[1,2048,896]{2,1,0:T(8,128)(2,1)} %param.33), kind=kOutput, calls=%fused_computation.10 | convolution fusion | flops 1879048192 | bytes 7602176 | tf_op jit(solution)/shard_map/dot_general | solution.py:568
  175.0 2.4 multiply_convert_fusion.1
  177.5 0.2 dot_general.31
  177.7 5.7 %fusion.21 = bf16[4,1,32,4,2048]{4,2,3,1,0:T(8,128)(2,1)} fusion(bf16[1,896,2048]{2,1,0:T(8,128)(2,1)} %param.35, bf16[4,32,4,896]{3,2,1,0:T(4,128)(2,1)S(1)} %dot_general.31), kind=kOutput, calls=%fused_computation.15 | convolution fusion | flops 1880096768 | bytes 6684672 | tf_op jit(solution)/shard_map/dot_general | solution.py:571
  183.4 4.5 %all-to-all-start.1 = ((bf16[4,1,32,4,2048]{4,2,3,1,0:T(8,128)(2,1)}), bf16[4,1,32,4,2048]{4,2,3,1,0:T(8,128)(2,1)}, u32[]{:S(2)}, u32[]{:S(2)}) async-start(bf16[4,1,32,4,2048]{4,2,3,1,0:T(8,128)(2,1)} %fusion.21), calls=%async_computation.1 | async-start | bytes 4194304 | tf_op jit(solution)/shard_map/all_to_all | solution.py:29
  187.9 12.8 %all-gather.5.cloned.1.call-done = bf16[128,4,2048]{2,1,0:T(4,128)(2,1)} async-done(((bf16[32,4,2048]{2,1,0:T(4,128)(2,1)}), bf16[128,4,2048]{2,1,0:T(4,128)(2,1)}) %all-gather.5.cloned.1.call-update) | async-done | bytes 2097168 | tf_op jit(solution)/shard_map/all_gather | solution.py:583
  200.8 2.5 reshape_reshape.7
  203.3 4.5 %fusion.8 = f32[512,896]{1,0:T(8,128)S(1)} fusion(bf16[512,2048]{1,0:T(8,128)(2,1)S(1)} %reshape_reshape.7, bf16[1,2048,896]{2,1,0:T(8,128)(2,1)} %param.33), kind=kOutput, calls=%fused_computation.8 | convolution fusion | flops 1879048192 | bytes 7602176 | tf_op jit(solution)/shard_map/dot_general | solution.py:568
  207.9 2.4 multiply_convert_fusion
  210.5 5.7 %fusion.18 = bf16[4,1,32,4,2048]{4,2,3,1,0:T(8,128)(2,1)} fusion(bf16[1,896,2048]{2,1,0:T(8,128)(2,1)} %param.35, bf16[4,32,4,896]{3,2,1,0:T(4,128)(2,1)S(1)} %dot_general.35), kind=kOutput, calls=%fused_computation.14 | convolution fusion | flops 1880096768 | bytes 6684672 | tf_op jit(solution)/shard_map/dot_general | solution.py:571
  216.2 3.1 all-to-all-done.1
  219.3 4.8 %all-to-all-start.3 = ((bf16[4,1,32,4,2048]{4,2,3,1,0:T(8,128)(2,1)}), bf16[4,1,32,4,2048]{4,2,3,1,0:T(8,128)(2,1)}, u32[]{:S(2)}, u32[]{:S(2)}) async-start(bf16[4,1,32,4,2048]{4,2,3,1,0:T(8,128)(2,1)} %fusion.18), calls=%async_computation.3 | async-start | bytes 4194304 | tf_op jit(solution)/shard_map/all_to_all | solution.py:29
  224.1 2.0 bitcast_reduce_fusion.1
  226.1 23.5 %all-to-all-done.3 = bf16[4,1,32,4,2048]{4,2,3,1,0:T(8,128)(2,1)} async-done(((bf16[4,1,32,4,2048]{4,2,3,1,0:T(8,128)(2,1)}), bf16[4,1,32,4,2048]{4,2,3,1,0:T(8,128)(2,1)}, u32[]{:S(2)}, u32[]{:S(2)}) %all-to-all-start.3) | async-done | bytes 2097184 | tf_op jit(solution)/shard_map/all_to_all | solution.py:29
  249.5 2.0 bitcast_reduce_fusion
  251.7 0.6 copy.86
  252.2 75.8 %all_to_all.27 = bf16[32,8,2048]{2,1,0:T(8,128)(2,1)S(1)} all-to-all(bf16[32,8,2048]{2,1,0:T(8,128)(2,1)S(1)} %copy.86), channel_id=1, replica_groups=mesh['grp'=2,'sp'=32,'tp'=4] {'sp'}, dimensions={0} | all-to-all | bytes 2097152 | tf_op jit(solution)/shard_map/all_to_all | solution.py:587
  328.0 0.4 fusion.29
  328.4 0.8 add_convert_fusion
  (55 shorter events, 2.0 us)
Async XLA Ops:
  6.5 5.5 %copy-start.9 = (f32[64]{0:T(128)S(1)}, f32[64]{0:T(128)}, u32[]{:S(2)}) copy-start(f32[64]{0:T(128)} %param.28) | copy-start | bytes 772
  6.5 5.5 %copy-start.10 = (f32[64]{0:T(128)S(1)}, f32[64]{0:T(128)}, u32[]{:S(2)}) copy-start(f32[64]{0:T(128)} %param.29) | copy-start | bytes 772
  6.6 161.4 %all-gather.3.cloned.1.call-start = ((), (), s32[]{:S(2)}) async-start(), calls=%async_computation.5 | async-start | bytes 2621440 | tf_op jit(solution)/shard_map/all_gather | solution.py:583
  6.8 6.1 %copy-start.11 = (f32[128]{0:T(128)S(1)}, f32[128]{0:T(128)}, u32[]{:S(2)}) copy-start(f32[128]{0:T(128)} %param.27) | copy-start | bytes 1540
  6.8 6.1 %copy-start.12 = (f32[128]{0:T(128)S(1)}, f32[128]{0:T(128)}, u32[]{:S(2)}) copy-start(f32[128]{0:T(128)} %param.26) | copy-start | bytes 1540
  6.8 6.1 %copy-start = (bf16[256,2048]{1,0:T(8,128)(2,1)S(1)}, bf16[256,2048]{1,0:T(8,128)(2,1)}, u32[]{:S(2)}) copy-start(bf16[256,2048]{1,0:T(8,128)(2,1)} %ow_hbm.1) | copy-start | bytes 3145732
  6.8 6.1 %copy-start.1 = (bf16[128,2048]{1,0:T(8,128)(2,1)S(1)}, bf16[128,2048]{1,0:T(8,128)(2,1)}, u32[]{:S(2)}) copy-start(bf16[128,2048]{1,0:T(8,128)(2,1)} %on_hbm.1) | copy-start | bytes 1572868
  6.8 6.1 %copy-start.2 = (bf16[64,2048]{1,0:T(8,128)(2,1)S(1)}, bf16[64,2048]{1,0:T(8,128)(2,1)}, u32[]{:S(2)}) copy-start(bf16[64,2048]{1,0:T(8,128)(2,1)} %res_ref.1) | copy-start | bytes 786436
  6.8 6.1 %copy-start.3 = (bf16[256,256]{1,0:T(8,128)(2,1)S(1)}, bf16[256,256]{1,0:T(8,128)(2,1)}, u32[]{:S(2)}) copy-start(bf16[256,256]{1,0:T(8,128)(2,1)} %qw_ref.1) | copy-start | bytes 393220
  6.8 6.1 %copy-start.4 = (bf16[256,128]{1,0:T(8,128)(2,1)S(1)}, bf16[256,128]{1,0:T(8,128)(2,1)}, u32[]{:S(2)}) copy-start(bf16[256,128]{1,0:T(8,128)(2,1)} %kw_ref.1) | copy-start | bytes 196612
  6.8 6.1 %copy-start.5 = (bf16[256,128]{1,0:T(8,128)(2,1)S(1)}, bf16[256,128]{1,0:T(8,128)(2,1)}, u32[]{:S(2)}) copy-start(bf16[256,128]{1,0:T(8,128)(2,1)} %vw_ref.1) | copy-start | bytes 196612
  6.9 6.1 %copy-start.6 = (bf16[256,128]{1,0:T(8,128)(2,1)S(1)}, bf16[256,128]{1,0:T(8,128)(2,1)}, u32[]{:S(2)}) copy-start(bf16[256,128]{1,0:T(8,128)(2,1)} %qn_ref.1) | copy-start | bytes 196612
  6.9 6.1 %copy-start.7 = (f32[2048]{0:T(1024)S(1)}, f32[2048]{0:T(1024)}, u32[]{:S(2)}) copy-start(f32[2048]{0:T(1024)} %param.32) | copy-start | bytes 24580
  130.3 70.5 %all-gather.5.cloned.1.call-start = ((), (), s32[]{:S(2)}) async-start(), calls=%async_computation.6 | async-start | bytes 2621440 | tf_op jit(solution)/shard_map/all_gather | solution.py:583
  170.5 4.5 %copy-start.13 = (bf16[1,2048,896]{2,1,0:T(8,128)(2,1)S(1)}, bf16[1,2048,896]{2,1,0:T(8,128)(2,1)}, u32[]{:S(2)}) copy-start(bf16[1,2048,896]{2,1,0:T(8,128)(2,1)} %param.34) | copy-start | bytes 11010052
  183.4 35.9 %all-to-all-start.1 = ((bf16[4,1,32,4,2048]{4,2,3,1,0:T(8,128)(2,1)}), bf16[4,1,32,4,2048]{4,2,3,1,0:T(8,128)(2,1)}, u32[]{:S(2)}, u32[]{:S(2)}) async-start(bf16[4,1,32,4,2048]{4,2,3,1,0:T(8,128)(2,1)} %fusion.21), calls=%async_computation.1 | async-start | bytes 4194304 | tf_op jit(solution)/shard_map/all_to_all | solution.py:29
  203.3 4.5 %copy-start.14 = (bf16[1,2048,896]{2,1,0:T(8,128)(2,1)S(1)}, bf16[1,2048,896]{2,1,0:T(8,128)(2,1)}, u32[]{:S(2)}) copy-start(bf16[1,2048,896]{2,1,0:T(8,128)(2,1)} %param.34) | copy-start | bytes 11010052
  219.3 30.2 %all-to-all-start.3 = ((bf16[4,1,32,4,2048]{4,2,3,1,0:T(8,128)(2,1)}), bf16[4,1,32,4,2048]{4,2,3,1,0:T(8,128)(2,1)}, u32[]{:S(2)}, u32[]{:S(2)}) async-start(bf16[4,1,32,4,2048]{4,2,3,1,0:T(8,128)(2,1)} %fusion.18), calls=%async_computation.3 | async-start | bytes 4194304 | tf_op jit(solution)/shard_map/all_to_all | solution.py:29
  251.6 76.4 %copy-start.8 = (f32[64,2]{0,1:T(2,128)S(1)}, f32[64,2]{0,1:T(2,128)}, u32[]{:S(2)}) copy-start(f32[64,2]{0,1:T(2,128)} %param.37) | copy-start | bytes 1540
Sparse Core Ops, SparseCore 0:
  130.4 27.5 all-gather.2
  168.0 32.7 all-gather.4

commit v2 on v1

--- a/solution.py
+++ b/solution.py
@@ -18,39 +18,6 @@
 BF16 = jnp.bfloat16
 
 
-def in_blocks(value, dim, peers):
-    lengths = value.shape
-    blocks = value.reshape(*lengths[:dim], peers, lengths[dim] // peers, *lengths[dim + 1 :])
-    return jnp.moveaxis(blocks, dim, 0)
-
-
-def sum_at_owner(value, axis, dim):
-    peers = lax.axis_size(axis)
-    blocks = lax.all_to_all(in_blocks(value, dim, peers), axis, 0, 0, tiled=True)
-    return jnp.sum(blocks.astype(jnp.float32), axis=0)
-
-
-def items_in_groups(value, axis, split_dim, concat_dim, work, item_dim, out_dim):
-    items = jax.tree.leaves(value)[0].shape[item_dim]
-    count = 2 if items % 2 == 0 else 1
-    finished = []
-    for k in range(count):
-        group = jax.tree.map(
-            lambda a: lax.slice_in_dim(
-                a, k * (items // count), (k + 1) * (items // count), axis=item_dim
-            ),
-            value,
-        )
-        finished.append(
-            work(
-                lax.all_to_all(
-                    group, axis, split_axis=split_dim, concat_axis=concat_dim, tiled=True
-                )
-            )
-        )
-    return jax.tree.map(lambda *parts: jnp.concatenate(parts, axis=out_dim), *finished)
-
-
 def angles_of(places, head_width):
     quarter = head_width // 4
     inv_freq = THETA ** (-jnp.arange(quarter, dtype=jnp.float32) / quarter)
@@ -94,7 +61,7 @@
     return values * scale * gain
 
 
-def attend_kernel(
+def layer_kernel(
     chips,
     peers,
     qw_ref,
@@ -106,10 +73,13 @@
     tables_ref,
     res_ref,
     norm_gain_ref,
+    route_ref,
     ow_hbm,
     on_hbm,
-    att_ref,
-    normed_ref,
+    gate_hbm,
+    up_hbm,
+    down_hbm,
+    out_ref,
     kv_buf,
     qws,
     qns,
@@ -122,13 +92,43 @@
     part,
     first_in,
     last_in,
+    info,
+    gate_buf,
+    up_buf,
+    down_buf,
+    att_buf,
+    rows_buf,
+    x_buf,
+    y_buf,
+    y_first,
+    y_last,
+    e_buf,
+    e_mate,
+    ret_out,
+    ret_in,
     w_sem,
     zsend,
     zrecv,
     psend,
     precv,
+    isend,
+    irecv,
+    imsend,
+    imrecv,
     xsend,
     xrecv,
+    z2send,
+    z2recv,
+    p2send,
+    p2recv,
+    asend,
+    arecv,
+    ysend,
+    yrecv,
+    esend,
+    erecv,
+    rsend,
+    rrecv,
 ):
     tok = qw_ref.shape[0]
     half = tok // 2
@@ -146,6 +146,9 @@
     w_copies = [
         pltpu.make_async_copy(ow_hbm, ow_buf, w_sem.at[0]),
         pltpu.make_async_copy(on_hbm, on_buf, w_sem.at[1]),
+        pltpu.make_async_copy(gate_hbm.at[0], gate_buf, w_sem.at[2]),
+        pltpu.make_async_copy(up_hbm.at[0], up_buf, w_sem.at[3]),
+        pltpu.make_async_copy(down_hbm.at[0], down_buf, w_sem.at[4]),
     ]
     for copy in w_copies:
         copy.start()
@@ -170,45 +173,70 @@
         lane_ids(kvn.shape) < wide // 2, k_narrow, kvn
     ).astype(BF16)
 
+    slots = 2 * 2 * res_ref.shape[0] // (2 * chips)
+    route = route_ref[...]
+    lanes = route.shape[1]
+    experts = lax.broadcasted_iota(jnp.int32, (2 * chips, lanes), 0).astype(F32)
+    hits = [(route[k : k + 1] == experts).astype(F32) for k in (0, 1)]
+    earlier = (
+        lax.broadcasted_iota(jnp.int32, (lanes, lanes), 0)
+        < lax.broadcasted_iota(jnp.int32, (lanes, lanes), 1)
+    ).astype(BF16)
+    places = jnp.dot((hits[0] + hits[1]).astype(BF16), earlier, preferred_element_type=F32)
+    targets = [
+        jnp.sum(hit * (places + experts * slots), axis=0, keepdims=True) for hit in hits
+    ]
+    row = lax.broadcasted_iota(jnp.int32, route.shape, 0)
+    info[sp] = jnp.where(row == 0, targets[0], jnp.where(row == 1, targets[1], route))
+
     pl.semaphore_wait(barrier, 5)
 
-    def z_copy(way, step, sub):
-        shift = step - 1
-        chip = (z + chips - shift) % chips if way == 0 else (z + shift) % chips
-        ref = rows_of(chip, core, sub)
+    def hop(src, dst, send, recv, device):
         return pltpu.make_async_remote_copy(
-            src_ref=ref,
-            dst_ref=ref,
-            send_sem=zsend.at[way, step - 1, sub],
-            recv_sem=zrecv.at[way, step - 1, sub],
-            device_id=right if way == 0 else left,
+            src_ref=src,
+            dst_ref=dst,
+            send_sem=send,
+            recv_sem=recv,
+            device_id=device,
             device_id_type=MESH,
         )
 
+    def same(ref, send, recv, device):
+        return hop(ref, ref, send, recv, device)
+
+    def chip_at(way, distance):
+        return (z + chips - distance) % chips if way == 0 else (z + distance) % chips
+
+    def along(way):
+        return right if way == 0 else left
+
+    def z_copy(way, step, sub):
+        ref = rows_of(chip_at(way, step - 1), core, sub)
+        return same(ref, zsend.at[way, step - 1, sub], zrecv.at[way, step - 1, sub], along(way))
+
     def z_arrival(way, step, sub):
-        chip = (z + chips - step) % chips if way == 0 else (z + step) % chips
-        ref = rows_of(chip, core, sub)
-        return pltpu.make_async_remote_copy(
-            src_ref=ref,
-            dst_ref=ref,
-            send_sem=zsend.at[way, step - 1, sub],
-            recv_sem=zrecv.at[way, step - 1, sub],
-            device_id=right if way == 0 else left,
-            device_id_type=MESH,
-        )
+        ref = rows_of(chip_at(way, step), core, sub)
+        return same(ref, zsend.at[way, step - 1, sub], zrecv.at[way, step - 1, sub], along(way))
 
     def m_copy(way, step, sub, owner):
-        chip = (z + chips - step) % chips if way == 0 else (z + step) % chips
-        ref = rows_of(chip, owner, sub)
-        return pltpu.make_async_remote_copy(
-            src_ref=ref,
-            dst_ref=ref,
-            send_sem=psend.at[way, step, sub],
-            recv_sem=precv.at[way, step, sub],
-            device_id=mate,
-            device_id_type=MESH,
-        )
-
+        ref = rows_of(chip_at(way, step), owner, sub)
+        return same(ref, psend.at[way, step, sub], precv.at[way, step, sub], mate)
+
+    def i_copy(way, step):
+        ref = info.at[chip_at(way, step - 1) * 2 + core]
+        return same(ref, isend.at[way, step - 1], irecv.at[way, step - 1], along(way))
+
+    def i_arrival(way, step):
+        ref = info.at[chip_at(way, step) * 2 + core]
+        return same(ref, isend.at[way, step - 1], irecv.at[way, step - 1], along(way))
+
+    def im_copy(way, step, owner):
+        ref = info.at[chip_at(way, step) * 2 + owner]
+        return same(ref, imsend.at[way, step], imrecv.at[way, step], mate)
+
+    for way in (0, 1):
+        i_copy(way, 1).start()
+    im_copy(0, 0, core).start()
     for way, sub in ((0, 0), (1, 1), (0, 1), (1, 0)):
         z_copy(way, 1, sub).start()
     for sub in (0, 1):
@@ -269,8 +297,18 @@
             acc_buf[at] = acc_buf[at] * alpha + mixed
 
     def ring_step(step, nothing):
+        def pass_on(way):
+            i_arrival(way, step).wait_recv()
+            if way == 0:
+                pl.when(step < far)(lambda: i_copy(way, step + 1).start())
+            else:
+                pl.when(step < far - 1)(lambda: i_copy(way, step + 1).start())
+            im_copy(way, step, core).start()
+
         @pl.when(step <= far)
         def _():
+            pass_on(0)
+            pl.when(step < far)(functools.partial(pass_on, 1))
             for turn in (0, 1):
                 for way in (0, 1):
                     sub = turn if way == 0 else 1 - turn
@@ -299,16 +337,19 @@
 
         @pl.when(before == 0)
         def _():
+            im_copy(0, 0, 1 - core).wait_recv()
             for sub in (0, 1):
                 m_copy(0, 0, sub, 1 - core).wait_recv()
 
         @pl.when(before > 0)
         def _():
+            im_copy(0, before, 1 - core).wait_recv()
             m_copy(0, before, 0, 1 - core).wait_recv()
             m_copy(1, before, 1, 1 - core).wait_recv()
 
         @pl.when(jnp.logical_and(before > 0, before < far))
         def _():
+            im_copy(1, before, 1 - core).wait_recv()
             m_copy(0, before, 1, 1 - core).wait_recv()
             m_copy(1, before, 0, 1 - core).wait_recv()
 
@@ -329,7 +370,7 @@
     heads[:, 2 * wide : 3 * wide] = jnp.where(
         low, pltpu.roll(outs[2], wide // 2, 1), outs[3]
     ).astype(BF16)
-    for copy in w_copies:
+    for copy in w_copies[:2]:
         copy.wait()
 
     rows = res_ref.shape[0]
@@ -385,31 +426,275 @@
     total = res_ref[...].astype(F32) + part[tp].astype(F32)
     total = total + last_in[0].astype(F32) + last_in[1].astype(F32)
     attended = total.astype(BF16)
-    att_ref[...] = attended
+    att_buf[...] = attended
     state = attended.astype(F32)
     mean = jnp.mean(state * state, axis=-1, keepdims=True)
-    normed_ref[...] = (state * lax.rsqrt(mean + EPS) * norm_gain_ref[...]).astype(BF16)
+    normed = (state * lax.rsqrt(mean + EPS) * norm_gain_ref[...]).astype(BF16)
+    rows_buf[pl.ds(pl.multiple_of(sp * rows, rows), rows)] = normed
+
+    def block_of(chip, owner, sub):
+        at = pl.multiple_of((chip * 2 + owner) * rows + sub * (rows // 2), rows // 2)
+        return rows_buf.at[pl.ds(at, rows // 2)]
+
+    def z2_copy(way, step, sub):
+        ref = block_of(chip_at(way, step - 1), core, sub)
+        return same(ref, z2send.at[way, step - 1, sub], z2recv.at[way, step - 1, sub], along(way))
+
+    def z2_arrival(way, step, sub):
+        ref = block_of(chip_at(way, step), core, sub)
+        return same(ref, z2send.at[way, step - 1, sub], z2recv.at[way, step - 1, sub], along(way))
+
+    def m2_copy(way, step, sub, owner):
+        ref = block_of(chip_at(way, step), owner, sub)
+        return same(ref, p2send.at[way, step, sub], p2recv.at[way, step, sub], mate)
+
+    for way, sub in ((0, 0), (1, 1), (0, 1), (1, 0)):
+        z2_copy(way, 1, sub).start()
+    for sub in (0, 1):
+        m2_copy(0, 0, sub, core).start()
+    for copy in w_copies[2:]:
+        copy.wait()
+
+    def beside(way):
+        return xright if way == 0 else xleft
+
+    def peer_at(way):
+        return (tp + 1) % peers if way == 0 else (tp + peers - 1) % peers
+
+    opposite = (tp + 2) % peers
+
+    def a_near(way, pair, owner):
+        return same(x_buf.at[pair, owner], asend.at[way, pair, 0], arecv.at[way, pair, 0], beside(way))
+
+    def a_far(way, pair, owner):
+        ref = x_buf.at[pair, owner, :, pl.ds(way * cols, cols)]
+        return same(ref, asend.at[way, pair, 1], arecv.at[way, pair, 1], beside(way))
+
+    def y_copy(way, pair, number):
+        with_far = way * cols
+        alone = (1 - way) * cols
+        if number == 0:
+            src = y_buf.at[pair, opposite, :, pl.ds(with_far, cols)]
+            dst = y_first.at[pair, way]
+        else:
+            at = pl.ds(alone if number == 1 else with_far, cols)
+            src = y_buf.at[pair, peer_at(way), :, at]
+            dst = y_last.at[pair, way, :, at]
+        return hop(src, dst, ysend.at[way, pair, number], yrecv.at[way, pair, number], beside(way))
+
+    def e_copy(pair):
+        return hop(
+            e_buf.at[pair, 1 - core], e_mate.at[pair], esend.at[pair], erecv.at[pair], mate
+        )
+
+    def ring_arrivals(step):
+        for turn in (0, 1):
+            for way in (0, 1):
+                sub = turn if way == 0 else 1 - turn
+
+                def arrived(way=way, sub=sub, turn=turn):
+                    z2_arrival(way, step, sub).wait_recv()
+                    last = far if turn == 0 else far - 1
+                    pl.when(step < last)(lambda: z2_copy(way, step + 1, sub).start())
+                    m2_copy(way, step, sub, core).start()
+
+                if turn == 0:
+                    arrived()
+                else:
+                    pl.when(step < far)(arrived)
+
+    def select(step):
+        pair = step % far
+        m2_copy(0, step, 0, 1 - core).wait_recv()
+        m2_copy(1, step, 1, 1 - core).wait_recv()
+
+        @pl.when(step < far)
+        def _():
+            m2_copy(0, step, 1, 1 - core).wait_recv()
+            m2_copy(1, step, 0, 1 - core).wait_recv()
+
+        @pl.when(step == far)
+        def _():
+            for sub in (0, 1):
+                m2_copy(0, 0, sub, 1 - core).wait_recv()
+
+        near = jnp.where(step == far, z, chip_at(0, step))
+        total = None
+        for number, (chip, owner) in enumerate(
+            ((near, 0), (chip_at(1, step), 0), (near, 1), (chip_at(1, step), 1))
+        ):
+            device = chip * 2 + owner
+            table = info[device]
+            slot = lax.broadcasted_iota(jnp.int32, (4 * slots, rows), 0)
+            want = jnp.where(slot // slots == number, sp * slots + slot % slots, -2).astype(F32)
+            hit = jnp.logical_or(table[0:1, 0:rows] == want, table[1:2, 0:rows] == want)
+            block = rows_buf[pl.ds(pl.multiple_of(device * rows, rows), rows)]
+            picked = jnp.dot(
+                jnp.where(hit, 1.0, 0.0).astype(BF16), block, preferred_element_type=F32
+            )
+            total = picked if total is None else total + picked
+        x_buf[pair, tp] = total.astype(BF16)
+        for way in (0, 1):
+            a_near(way, pair, tp).start()
+
+    def forward(step):
+        pair = step % far
+        for way in (0, 1):
+            source = peer_at(1 - way)
+            a_near(way, pair, source).wait_recv()
+            a_far(way, pair, source).start()
+
+    def run_expert(step):
+        pair = step % far
+        for way in (0, 1):
+            a_far(way, pair, opposite).wait_recv()
+        x = x_buf[pair].reshape(peers * 4 * slots, 2 * cols)
+        gate = jnp.dot(x, gate_buf[...], preferred_element_type=F32)
+        up = jnp.dot(x, up_buf[...], preferred_element_type=F32)
+        hidden = (gate / (1.0 + jnp.exp(-gate)) * up).astype(BF16)
+        y = jnp.dot(hidden, down_buf[...], preferred_element_type=F32)
+        y_buf[pair] = y.astype(BF16).reshape(peers, 4 * slots, 2 * cols)
+        for number in (0, 1):
+            for way in (0, 1):
+                y_copy(way, pair, number).start()
+
+    def add_far(step):
+        pair = step % far
+        for way in (0, 1):
+            y_copy(way, pair, 0).wait_recv()
+            at = slice(way * cols, (way + 1) * cols)
+            y_buf[pair, peer_at(way), :, at] = (
+                y_buf[pair, peer_at(way), :, at].astype(F32) + y_first[pair, way].astype(F32)
+            ).astype(BF16)
+            y_copy(way, pair, 2).start()
+
+    def finish(step):
+        pair = step % far
+        for way in (0, 1):
+            y_copy(way, pair, 1).wait_recv()
+            y_copy(way, pair, 2).wait_recv()
+        total = y_buf[pair, tp].astype(F32)
+        total = total + y_last[pair, 0].astype(F32) + y_last[pair, 1].astype(F32)
+        e_buf[pair] = total.astype(BF16).reshape(2, 2 * slots, 2 * cols)
+        e_copy(pair).start()
+
+    stages = (ring_arrivals, select, forward, run_expert, add_far, finish)
+
+    def tick(at, nothing):
+        for lag, stage in enumerate(stages):
+            step = at - lag
+            pl.when(jnp.logical_and(step >= 1, step <= far))(functools.partial(stage, step))
+        return nothing
+
+    lax.fori_loop(1, far + len(stages), tick, 0)
+
+    def contribution(chip, pair, which, sub):
+        table = info[chip * 2 + core]
+        slot = lax.broadcasted_iota(jnp.int32, (4 * slots, rows), 0)
+        expert = jnp.where(slot < 2 * slots, sp, z * 2 + (1 - core))
+        ours = (slot % (2 * slots)) // slots == which
+        want = jnp.where(ours, expert * slots + slot % slots, -2).astype(F32)
+        weight = jnp.where(table[0:1, 0:rows] == want, table[2:3, 0:rows], 0.0)
+        weight = weight + jnp.where(table[1:2, 0:rows] == want, table[3:4, 0:rows], 0.0)
+        coarse = weight.astype(BF16)
+        fine = (weight - coarse.astype(F32)).astype(BF16)
+        at = slice(sub * cols, (sub + 1) * cols)
+        mine, other = e_buf[pair, core, :, at], e_mate[pair, :, at]
+        return lax.dot_general(
+            jnp.concatenate([coarse, fine], axis=0),
+            jnp.concatenate([mine, other, mine, other], axis=0),
+            (((0,), (0,)), ((), ())),
+            preferred_element_type=F32,
+        )
+
+    def r_copy(way, step, sub):
+        at = pl.ds(sub * cols, cols)
+        return hop(
+            ret_out.at[way, step, :, at],
+            ret_in.at[way, step, :, at],
+            rsend.at[way, step, sub],
+            rrecv.at[way, step, sub],
+            along(way),
+        )
+
+    e_copy(0).wait_recv()
+    for way in (0, 1):
+        at = slice(way * cols, (way + 1) * cols)
+        ret_out[way, 0, :, at] = contribution((z + far) % chips, 0, 1, way).astype(BF16)
+        r_copy(way, 0, way).start()
+        rest = slice((1 - way) * cols, (2 - way) * cols)
+        ret_in[way, 0, :, rest] = jnp.zeros((rows, cols), BF16)
+
+    def back_step(step, nothing):
+        distance = far - step
+        e_copy(distance).wait_recv()
+        for turn in (0, 1):
+            for way in (0, 1):
+                sub = turn if way == 0 else 1 - turn
+                added = contribution(chip_at(1 - way, distance), distance, 1 - way, sub)
+                if turn == 0:
+                    r_copy(way, step - 1, sub).wait_recv()
+                else:
+                    pl.when(step > 1)(lambda: r_copy(way, step - 1, sub).wait_recv())
+                at = slice(sub * cols, (sub + 1) * cols)
+                ret_out[way, step, :, at] = (
+                    added + ret_in[way, step - 1, :, at].astype(F32)
+                ).astype(BF16)
+                r_copy(way, step, sub).start()
+        return nothing
+
+    lax.fori_loop(1, far, back_step, 0)
+    for sub in (0, 1):
+        at = slice(sub * cols, (sub + 1) * cols)
+        total = att_buf[:, at].astype(F32) + contribution(z, 0, 0, sub)
+        for way in (0, 1):
+            r_copy(way, far - 1, sub).wait_recv()
+            total = total + ret_in[way, far - 1, :, at].astype(F32)
+        out_ref[:, at] = total.astype(BF16)
 
     for way in (0, 1):
         for number in (0, 1, 2):
             x_copy(way, number).wait_send()
     for sub in (0, 1):
         m_copy(0, 0, sub, core).wait_send()
+        m2_copy(0, 0, sub, core).wait_send()
+    im_copy(0, 0, core).wait_send()
 
     def drain(step, nothing):
         for way in (0, 1):
+            i_copy(way, step).wait_send()
+            im_copy(way, step, core).wait_send()
             for sub in (0, 1):
                 z_copy(way, step, sub).wait_send()
                 m_copy(way, step, sub, core).wait_send()
+                z2_copy(way, step, sub).wait_send()
+                m2_copy(way, step, sub, core).wait_send()
+                r_copy(way, step, sub).wait_send()
         return nothing
 
     lax.fori_loop(1, far, drain, 0)
+    i_copy(0, far).wait_send()
+    im_copy(0, far, core).wait_send()
     for way in (0, 1):
         z_copy(way, far, way).wait_send()
         m_copy(way, far, way, core).wait_send()
-
-
-def attend(
+        z2_copy(way, far, way).wait_send()
+        m2_copy(way, far, way, core).wait_send()
+        r_copy(way, 0, way).wait_send()
+
+    def drain_pairs(pair, nothing):
+        e_copy(pair).wait_send()
+        for way in (0, 1):
+            a_near(way, pair, tp).wait_send()
+            a_far(way, pair, peer_at(1 - way)).wait_send()
+            for number in (0, 1, 2):
+                y_copy(way, pair, number).wait_send()
+        return nothing
+
+    lax.fori_loop(0, far, drain_pairs, 0)
+
+
+def layer(
     residual,
     queries_wide,
     keys_wide,
@@ -420,25 +705,27 @@
     gains,
     tables,
     norm_gain,
+    route,
     output_wide,
     output_narrow,
+    gate_weight,
+    up_weight,
+    down_weight,
 ):
     chips = lax.axis_size("sp") // 2
     peers = lax.axis_size("tp")
     tok, wide = keys_wide.shape
     rows, width = residual.shape
     far = chips // 2
+    picked = 4 * (2 * 2 * rows // (2 * chips))
     vmem = pl.BlockSpec(memory_space=pltpu.VMEM)
     hbm = pl.BlockSpec(memory_space=pl.ANY)
     dma = pltpu.SemaphoreType.DMA
     return pl.pallas_call(
-        functools.partial(attend_kernel, chips, peers),
-        out_shape=(
-            jax.ShapeDtypeStruct((rows, width), BF16),
-            jax.ShapeDtypeStruct((rows, width), BF16),
-        ),
-        in_specs=[vmem] * 9 + [hbm] * 2,
-        out_specs=(vmem, vmem),
+        functools.partial(layer_kernel, chips, peers),
+        out_shape=jax.ShapeDtypeStruct((rows, width), BF16),
+        in_specs=[vmem] * 10 + [hbm] * 5,
+        out_specs=vmem,
         scratch_shapes=[
             pltpu.VMEM((2 * chips * tok, 3 * wide), BF16),
             pltpu.VMEM((2 * tok, wide), BF16),
@@ -452,18 +739,48 @@
             pltpu.VMEM((peers, rows, width), BF16),
             pltpu.VMEM((2, rows, width // 2), BF16),
             pltpu.VMEM((2, rows, width), BF16),
-            dma((2,)),
+            pltpu.VMEM((2 * chips,) + route.shape, F32),
+            pltpu.VMEM(gate_weight.shape[1:], BF16),
+            pltpu.VMEM(up_weight.shape[1:], BF16),
+            pltpu.VMEM(down_weight.shape[1:], BF16),
+            pltpu.VMEM((rows, width), BF16),
+            pltpu.VMEM((2 * chips * rows, width), BF16),
+            pltpu.VMEM((far, peers, picked, width), BF16),
+            pltpu.VMEM((far, peers, picked, width), BF16),
+            pltpu.VMEM((far, 2, picked, width // 2), BF16),
+            pltpu.VMEM((far, 2, picked, width), BF16),
+            pltpu.VMEM((far, 2, picked // 2, width), BF16),
+            pltpu.VMEM((far, picked // 2, width), BF16),
+            pltpu.VMEM((2, far, rows, width), BF16),
+            pltpu.VMEM((2, far, rows, width), BF16),
+            dma((5,)),
             dma((2, far, 2)),
             dma((2, far, 2)),
             dma((2, far + 1, 2)),
             dma((2, far + 1, 2)),
+            dma((2, far)),
+            dma((2, far)),
+            dma((2, far + 1)),
+            dma((2, far + 1)),
             dma((2, 3)),
             dma((2, 3)),
+            dma((2, far, 2)),
+            dma((2, far, 2)),
+            dma((2, far + 1, 2)),
+            dma((2, far + 1, 2)),
+            dma((2, far, 2)),
+            dma((2, far, 2)),
+            dma((2, far, 3)),
+            dma((2, far, 3)),
+            dma((far,)),
+            dma((far,)),
+            dma((2, far, 2)),
+            dma((2, far, 2)),
         ],
         compiler_params=pltpu.CompilerParams(
-            collective_id=0, has_side_effects=True, vmem_limit_bytes=40 * 1024 * 1024
+            collective_id=0, has_side_effects=True, vmem_limit_bytes=64 * 1024 * 1024 - 65536
         ),
-        name="attend",
+        name="layer",
     )(
         queries_wide,
         keys_wide,
@@ -474,23 +791,13 @@
         tables,
         residual,
         norm_gain.reshape(1, width),
+        route,
         output_wide,
         output_narrow,
+        gate_weight,
+        up_weight,
+        down_weight,
     )
-
-
-def slot_tables(chosen, slot_count, expert_count):
-    row_count = chosen.shape[0]
-    pick_count = chosen.shape[1]
-    flat_pick = chosen.reshape(row_count * pick_count)
-    hit_marks = (flat_pick[:, None] == jnp.arange(expert_count, dtype=jnp.int32)[None, :]).astype(
-        jnp.int32
-    )
-    before = jnp.cumsum(hit_marks, axis=0) - hit_marks
-    slot_place = jnp.sum(before * hit_marks, axis=1)
-    target = flat_pick * slot_count + slot_place
-    slot_table = target[:, None] == jnp.arange(expert_count * slot_count, dtype=jnp.int32)[None, :]
-    return slot_table.astype(jnp.bfloat16).reshape(row_count, pick_count, expert_count * slot_count)
 
 
 def body(
@@ -540,7 +847,10 @@
             jnp.concatenate([key_gain_narrow, key_gain_narrow]),
         ]
     )
-    attended, normed = attend(
+    own_rows = residual.shape[0]
+    route = jnp.concatenate([route_ids.astype(F32), route_weights], axis=1).T
+    route = jnp.pad(route, ((0, 4), (0, 128 - own_rows)), constant_values=-1.0)
+    return layer(
         residual,
         queries_wide,
         keys_wide,
@@ -551,46 +861,13 @@
         gains,
         tables,
         norm_gain,
+        route,
         output_wide,
         output_narrow,
+        gate_weight,
+        up_weight,
+        down_weight,
     )
-    own_rows = residual.shape[0]
-    state_float = attended.astype(jnp.float32)
-    pick_count = route_ids.shape[1]
-    expert_count = lax.axis_size("sp")
-    slot_count = 2 * pick_count * own_rows // expert_count
-    model_width = residual.shape[1]
-    own_tables = slot_tables(route_ids, slot_count, expert_count)
-
-    def expert_block(arrived):
-        full_shape = arrived.shape
-        flat_rows = arrived.reshape(-1, model_width)
-        gate_act = jnp.dot(flat_rows, gate_weight[0], preferred_element_type=jnp.float32)
-        up_act = jnp.dot(flat_rows, up_weight[0], preferred_element_type=jnp.float32)
-        hidden = (jax.nn.silu(gate_act) * up_act).astype(jnp.bfloat16)
-        partial_value = jnp.dot(hidden, down_weight[0], preferred_element_type=jnp.float32).reshape(
-            full_shape
-        )
-        summed = sum_at_owner(partial_value.astype(jnp.bfloat16), "tp", 0)
-        return summed.reshape(full_shape[1:]).astype(jnp.bfloat16)
-
-    send_rows = jnp.einsum(
-        "rks,rd->sd", own_tables, normed, preferred_element_type=jnp.float32
-    ).astype(jnp.bfloat16)
-    send_rows = send_rows.reshape(expert_count, slot_count, model_width)
-
-    def copy_then_run(arrived):
-        copies = lax.all_gather(arrived, "tp", axis=0, tiled=True)
-        return expert_block(copies.reshape((lax.axis_size("tp"),) + arrived.shape))
-
-    results = items_in_groups(send_rows, "sp", 0, 0, copy_then_run, 1, 1)
-    returned = lax.all_to_all(results, "sp", split_axis=0, concat_axis=0, tiled=True)
-    returned_flat = returned.reshape(expert_count * slot_count, model_width)
-    picked = jnp.einsum(
-        "rks,sd->rkd", own_tables, returned_flat, preferred_element_type=jnp.float32
-    )
-    mixture = jnp.sum(route_weights[:, :, None] * picked, axis=1)
-    return (state_float + mixture).astype(jnp.bfloat16)
 
 
 def solution(mesh):

time: 337 us -> 225 us (0.67)
  blocking collectives: 153 us -> 0 us
  Pallas kernels: 76.6 us -> 219 us
  waiting for transfers between devices: 39.5 us -> 0 us
  matrix products: 26.1 us -> 0 us
  between operations: 13.9 us -> 0.14 us
  starting transfers between devices: 9.34 us -> 0 us
  local copies, waits for them, and re-layouts: 9.82 us -> 2.85 us
  other arithmetic: 7.59 us -> 3.59 us
    all_to_all x3 -> x0, blocking collectives: 153 us -> none  [the longest x2 77.3 us: items_in_groups(): lax.all_to_all(group, axis, split_axis=split_dim, concat_axis=concat_dim,...]
    pallas_call x1, Pallas kernels: 76.6 us -> 219 us  [layer(): pl.pallas_call(functools.partial(layer_kernel, chips, peers), out_shape=j...]
    all_to_all x2 -> x0, waiting for transfers between devices: 26.6 us -> none  [sum_at_owner(): lax.all_to_all(in_blocks(value, dim, peers), axis, 0, 0, tiled=True)]
    dot_general x8 -> x0, matrix products: 26.1 us -> none  [the longest x2 11.4 us: expert_block(): jnp.dot(hidden, down_weight[0], preferred_element_type=jnp.float32)]
    all_gather x2 -> x0, waiting for transfers between devices: 12.9 us -> none  [copy_then_run(): copies = lax.all_gather(arrived, 'tp', axis=0, tiled=True)]
    all_to_all x2 -> x0, starting transfers between devices: 9.28 us -> none  [sum_at_owner(): lax.all_to_all(in_blocks(value, dim, peers), axis, 0, 0, tiled=True)]
    another operation x2 -> x0, local copies, waits for them, and re-layouts: 5.07 us -> none  [expert_block(): flat_rows = arrived.reshape(-1, model_width)]
    reduce_sum x4 -> x0, other arithmetic: 4.24 us -> none  [the longest x2 3.98 us: sum_at_owner(): return jnp.sum(blocks.astype(jnp.float32), axis=0)]
  transfers between devices with their start and end apart: 4 -> 0, of which waited for: 3 -> 0; matrix products, arithmetic and copies ran while one was open for 10% -> 0% of each run, Pallas kernels for 0% -> 0%
where the time goes in v2:
time: 225 us
  Pallas kernels  219 us (97%)
  other arithmetic  3.59 us (2%)
  local copies, waits for them, and re-layouts  2.85 us (1%)
    pallas_call x1, Pallas kernels, layer(): pl.pallas_call(functools.partial(layer_kernel, chips, peers), out_shape=j...  219 us

profile of v2, /device:TPU:33, one launch (start us, length us, event | category | flops | bytes accessed | tf_op | source)
XLA Modules:
  0.0 225.2 jit_solution(2688416514839078431)
XLA Ops:
  0.0 0.0 copy-start.4
  0.0 0.0 copy-start.5
  0.0 0.0 copy-start.7
  0.0 0.0 copy-start.6
  0.0 0.0 copy-start
  0.0 0.0 copy-start.1
  0.0 0.0 copy-start.2
  0.0 0.0 copy-start.3
  0.1 0.1 multiply_bitcast_fusion
  0.2 0.3 concatenate.64
  0.6 0.5 fusion.4
  1.1 0.1 multiply_bitcast_fusion.3
  1.2 0.6 fusion
  1.8 0.8 pad_maximum_fusion.tables_ref
  2.6 0.0 copy-done.4
  2.6 0.0 copy-done.5
  2.6 0.1 maximum_bitcast_fusion.1
  2.7 0.0 copy-done.7
  2.7 0.0 copy-done.6
  2.7 0.6 pad_maximum_fusion.3.gains_ref
  3.3 0.0 copy-done
  3.3 0.1 copy.20
  3.4 0.0 copy-done.1
  3.4 0.1 copy.21
  3.5 0.7 pad_maximum_fusion.2.kvn_ref
  4.3 0.0 copy-done.2
  4.3 0.0 copy-done.3
  4.3 0.6 pad.4.route_ref
  4.9 218.7 %layer.1 = bf16[64,2048]{1,0:T(8,128)(2,1)} custom-call(bf16[256,256]{1,0:T(8,128)(2,1)} %qw_ref.1, bf16[256,128]{1,0:T(8,128)(2,1)} %kw_ref.1, bf16[256,128]{1,0:T(8,128)(2,1)} %vw_ref.1, bf16[256,128]{1,0:T(8,128)(2,1)} %qn_ref.1, bf16[256,128]{1,0:T(8,128)(2,1)} %pad_maximum_fusion.2.kvn_ref, f32[4,128]{1,0:T(4,128)} %pad_maximum_fusion.3.gains_ref, ...), custom_call_target="tpu_custom_call" | custom-call | tf_op jit(solution)/shard_map/layer/pallas_call | solution.py:724
  223.6 1.7 copy.23
  (7 shorter events, 0.1 us)
Async XLA Ops:
  0.0 2.6 %copy-start.4 = (f32[64]{0:T(128)S(1)}, f32[64]{0:T(128)}, u32[]{:S(2)}) copy-start(f32[64]{0:T(128)} %param.28) | copy-start | bytes 772
  0.0 2.6 %copy-start.5 = (f32[64]{0:T(128)S(1)}, f32[64]{0:T(128)}, u32[]{:S(2)}) copy-start(f32[64]{0:T(128)} %param.29) | copy-start | bytes 772
  0.0 2.7 %copy-start.7 = (f32[128]{0:T(128)S(1)}, f32[128]{0:T(128)}, u32[]{:S(2)}) copy-start(f32[128]{0:T(128)} %param.26) | copy-start | bytes 1540
  0.0 2.7 %copy-start.6 = (f32[128]{0:T(128)S(1)}, f32[128]{0:T(128)}, u32[]{:S(2)}) copy-start(f32[128]{0:T(128)} %param.27) | copy-start | bytes 1540
  0.0 3.3 %copy-start = (bf16[256,64]{0,1:T(8,128)(2,1)S(1)}, bf16[256,64]{0,1:T(8,128)(2,1)}, u32[]{:S(2)}) copy-start(bf16[256,64]{0,1:T(8,128)(2,1)} %param.24) | copy-start | bytes 98308
  0.0 3.4 %copy-start.1 = (bf16[256,64]{0,1:T(8,128)(2,1)S(1)}, bf16[256,64]{0,1:T(8,128)(2,1)}, u32[]{:S(2)}) copy-start(bf16[256,64]{0,1:T(8,128)(2,1)} %param.25) | copy-start | bytes 98308
  0.0 4.2 %copy-start.2 = (s32[64,2]{0,1:T(2,128)S(1)}, s32[64,2]{0,1:T(2,128)}, u32[]{:S(2)}) copy-start(s32[64,2]{0,1:T(2,128)} %param.36) | copy-start | bytes 1540
  0.0 4.2 %copy-start.3 = (f32[64,2]{0,1:T(2,128)S(1)}, f32[64,2]{0,1:T(2,128)}, u32[]{:S(2)}) copy-start(f32[64,2]{0,1:T(2,128)} %param.37) | copy-start | bytes 1540

commit v3 on v2

--- a/solution.py
+++ b/solution.py
@@ -554,6 +554,10 @@
         hidden = (gate / (1.0 + jnp.exp(-gate)) * up).astype(BF16)
         y = jnp.dot(hidden, down_buf[...], preferred_element_type=F32)
         y_buf[pair] = y.astype(BF16).reshape(peers, 4 * slots, 2 * cols)
+        pl.when(step >= far - 1)(lambda: begin_sum(step))
+
+    def begin_sum(step):
+        pair = step % far
         for number in (0, 1):
             for way in (0, 1):
                 y_copy(way, pair, number).start()
@@ -578,7 +582,7 @@
         e_buf[pair] = total.astype(BF16).reshape(2, 2 * slots, 2 * cols)
         e_copy(pair).start()
 
-    stages = (ring_arrivals, select, forward, run_expert, add_far, finish)
+    stages = (ring_arrivals, select, forward, run_expert)
 
     def tick(at, nothing):
         for lag, stage in enumerate(stages):
@@ -617,17 +621,18 @@
             along(way),
         )
 
-    e_copy(0).wait_recv()
     for way in (0, 1):
-        at = slice(way * cols, (way + 1) * cols)
-        ret_out[way, 0, :, at] = contribution((z + far) % chips, 0, 1, way).astype(BF16)
-        r_copy(way, 0, way).start()
         rest = slice((1 - way) * cols, (2 - way) * cols)
         ret_in[way, 0, :, rest] = jnp.zeros((rows, cols), BF16)
 
-    def back_step(step, nothing):
-        distance = far - step
-        e_copy(distance).wait_recv()
+    def start_back():
+        for way in (0, 1):
+            at = slice(way * cols, (way + 1) * cols)
+            ret_out[way, 0, :, at] = contribution((z + far) % chips, 0, 1, way).astype(BF16)
+            r_copy(way, 0, way).start()
+
+    def go_back(distance):
+        step = far - distance
         for turn in (0, 1):
             for way in (0, 1):
                 sub = turn if way == 0 else 1 - turn
@@ -641,9 +646,22 @@
                     added + ret_in[way, step - 1, :, at].astype(F32)
                 ).astype(BF16)
                 r_copy(way, step, sub).start()
+
+    def back(distance):
+        e_copy(distance % far).wait_recv()
+        pl.when(distance == far)(start_back)
+        pl.when(distance < far)(functools.partial(go_back, distance))
+
+    back_stages = ((2, back), (1, finish), (0, add_far), (-2, begin_sum))
+
+    def back_tick(at, nothing):
+        for lag, stage in back_stages:
+            step = far - at + lag
+            last = far - 2 if stage is begin_sum else far
+            pl.when(jnp.logical_and(step >= 1, step <= last))(functools.partial(stage, step))
         return nothing
 
-    lax.fori_loop(1, far, back_step, 0)
+    lax.fori_loop(0, far + 2, back_tick, 0)
     for sub in (0, 1):
         at = slice(sub * cols, (sub + 1) * cols)
         total = att_buf[:, at].astype(F32) + contribution(z, 0, 0, sub)

time: 225 us -> 208 us (0.924)
  Pallas kernels: 219 us -> 202 us
    pallas_call x1, Pallas kernels: 219 us -> 202 us  [layer(): pl.pallas_call(functools.partial(layer_kernel, chips, peers), out_shape=j...]
where the time goes in v3:
time: 208 us
  Pallas kernels  202 us (97%)
  other arithmetic  3.59 us (2%)
  local copies, waits for them, and re-layouts  2.85 us (1%)
    pallas_call x1, Pallas kernels, layer(): pl.pallas_call(functools.partial(layer_kernel, chips, peers), out_shape=j...  202 us

profile of v3, /device:TPU:33, one launch (start us, length us, event | category | flops | bytes accessed | tf_op | source)
XLA Modules:
  0.0 208.3 jit_solution(600312753026637974)
XLA Ops:
  0.0 0.0 copy-start.4
  0.0 0.0 copy-start.5
  0.0 0.0 copy-start.7
  0.0 0.0 copy-start.6
  0.0 0.0 copy-start
  0.0 0.0 copy-start.1
  0.0 0.0 copy-start.2
  0.0 0.0 copy-start.3
  0.1 0.1 multiply_bitcast_fusion
  0.2 0.3 concatenate.64
  0.6 0.5 fusion.4
  1.1 0.1 multiply_bitcast_fusion.3
  1.2 0.6 fusion
  1.8 0.8 pad_maximum_fusion.tables_ref
  2.6 0.0 copy-done.4
  2.6 0.0 copy-done.5
  2.6 0.1 maximum_bitcast_fusion.1
  2.7 0.0 copy-done.7
  2.7 0.0 copy-done.6
  2.7 0.6 pad_maximum_fusion.3.gains_ref
  3.3 0.0 copy-done
  3.3 0.1 copy.20
  3.4 0.0 copy-done.1
  3.4 0.1 copy.21
  3.5 0.7 pad_maximum_fusion.2.kvn_ref
  4.3 0.0 copy-done.2
  4.3 0.0 copy-done.3
  4.3 0.6 pad.4.route_ref
  4.9 201.7 %layer.1 = bf16[64,2048]{1,0:T(8,128)(2,1)} custom-call(bf16[256,256]{1,0:T(8,128)(2,1)} %qw_ref.1, bf16[256,128]{1,0:T(8,128)(2,1)} %kw_ref.1, bf16[256,128]{1,0:T(8,128)(2,1)} %vw_ref.1, bf16[256,128]{1,0:T(8,128)(2,1)} %qn_ref.1, bf16[256,128]{1,0:T(8,128)(2,1)} %pad_maximum_fusion.2.kvn_ref, f32[4,128]{1,0:T(4,128)} %pad_maximum_fusion.3.gains_ref, ...), custom_call_target="tpu_custom_call" | custom-call | tf_op jit(solution)/shard_map/layer/pallas_call | solution.py:742
  206.6 1.7 copy.23
  (7 shorter events, 0.1 us)
Async XLA Ops:
  0.0 2.6 %copy-start.4 = (f32[64]{0:T(128)S(1)}, f32[64]{0:T(128)}, u32[]{:S(2)}) copy-start(f32[64]{0:T(128)} %param.28) | copy-start | bytes 772
  0.0 2.6 %copy-start.5 = (f32[64]{0:T(128)S(1)}, f32[64]{0:T(128)}, u32[]{:S(2)}) copy-start(f32[64]{0:T(128)} %param.29) | copy-start | bytes 772
  0.0 2.7 %copy-start.7 = (f32[128]{0:T(128)S(1)}, f32[128]{0:T(128)}, u32[]{:S(2)}) copy-start(f32[128]{0:T(128)} %param.26) | copy-start | bytes 1540
  0.0 2.7 %copy-start.6 = (f32[128]{0:T(128)S(1)}, f32[128]{0:T(128)}, u32[]{:S(2)}) copy-start(f32[128]{0:T(128)} %param.27) | copy-start | bytes 1540
  0.0 3.3 %copy-start = (bf16[256,64]{0,1:T(8,128)(2,1)S(1)}, bf16[256,64]{0,1:T(8,128)(2,1)}, u32[]{:S(2)}) copy-start(bf16[256,64]{0,1:T(8,128)(2,1)} %param.24) | copy-start | bytes 98308
  0.0 3.4 %copy-start.1 = (bf16[256,64]{0,1:T(8,128)(2,1)S(1)}, bf16[256,64]{0,1:T(8,128)(2,1)}, u32[]{:S(2)}) copy-start(bf16[256,64]{0,1:T(8,128)(2,1)} %param.25) | copy-start | bytes 98308
  0.0 4.2 %copy-start.2 = (s32[64,2]{0,1:T(2,128)S(1)}, s32[64,2]{0,1:T(2,128)}, u32[]{:S(2)}) copy-start(s32[64,2]{0,1:T(2,128)} %param.36) | copy-start | bytes 1540
  0.0 4.2 %copy-start.3 = (f32[64,2]{0,1:T(2,128)S(1)}, f32[64,2]{0,1:T(2,128)}, u32[]{:S(2)}) copy-start(f32[64,2]{0,1:T(2,128)} %param.37) | copy-start | bytes 1540

commit v4 on v3

--- a/solution.py
+++ b/solution.py
@@ -9,6 +9,7 @@
 from jax.sharding import PartitionSpec as P
 
 GRID = 64
+FAR_STEPS = 3
 THETA = 10000.0
 EPS = 1e-06
 NEG_BIG = -1e30
@@ -106,6 +107,12 @@
     e_mate,
     ret_out,
     ret_in,
+    c_out,
+    c_in,
+    c_mate,
+    own_rows,
+    g_out,
+    g_in,
     w_sem,
     zsend,
     zrecv,
@@ -129,6 +136,12 @@
     erecv,
     rsend,
     rrecv,
+    csend,
+    crecv,
+    cmsend,
+    cmrecv,
+    gsend,
+    grecv,
 ):
     tok = qw_ref.shape[0]
     half = tok // 2
@@ -487,55 +500,146 @@
             e_buf.at[pair, 1 - core], e_mate.at[pair], esend.at[pair], erecv.at[pair], mate
         )
 
-    def ring_arrivals(step):
+    tile = 2 * slots
+    near = far - FAR_STEPS
+
+    def c_copy(way, number, piece):
+        last = FAR_STEPS - 1
+        if piece == 0:
+            at = (pl.ds(number * tile, (last - number) * tile),)
+        else:
+            at = (pl.ds(last * tile, tile), pl.ds(way * cols, cols))
+        src = c_out.at[way] if number == 0 else c_in.at[way, number - 1]
+        return hop(
+            src.at[at],
+            c_in.at[(way, number) + at],
+            csend.at[way, number, piece],
+            crecv.at[way, number, piece],
+            along(way),
+        )
+
+    def cm_copy(way, number):
+        at = (pl.ds(number * tile, tile),)
+        to = ()
+        if number == FAR_STEPS - 1:
+            at = at + (pl.ds(way * cols, cols),)
+            to = (slice(None), pl.ds(way * cols, cols))
+        return hop(
+            c_in.at[(way, number) + at],
+            c_mate.at[(way, number) + to],
+            cmsend.at[way, number],
+            cmrecv.at[way, number],
+            mate,
+        )
+
+    def pieces_of(number):
+        return (0, 1) if number < FAR_STEPS - 1 else (1,)
+
+    def picks(table, want):
+        hit = jnp.logical_or(table[0:1, 0:rows] == want, table[1:2, 0:rows] == want)
+        return jnp.where(hit, 1.0, 0.0).astype(BF16)
+
+    def rows_at(device):
+        return rows_buf[pl.ds(pl.multiple_of(device * rows, rows), rows)]
+
+    def near_arrivals(step):
         for turn in (0, 1):
             for way in (0, 1):
                 sub = turn if way == 0 else 1 - turn
-
-                def arrived(way=way, sub=sub, turn=turn):
-                    z2_arrival(way, step, sub).wait_recv()
-                    last = far if turn == 0 else far - 1
-                    pl.when(step < last)(lambda: z2_copy(way, step + 1, sub).start())
-                    m2_copy(way, step, sub, core).start()
-
-                if turn == 0:
-                    arrived()
-                else:
-                    pl.when(step < far)(arrived)
-
-    def select(step):
-        pair = step % far
-        m2_copy(0, step, 0, 1 - core).wait_recv()
-        m2_copy(1, step, 1, 1 - core).wait_recv()
-
-        @pl.when(step < far)
+                z2_arrival(way, step, sub).wait_recv()
+                pl.when(step < near)(lambda: z2_copy(way, step + 1, sub).start())
+                m2_copy(way, step, sub, core).start()
+
+        @pl.when(step == near)
         def _():
-            m2_copy(0, step, 1, 1 - core).wait_recv()
-            m2_copy(1, step, 0, 1 - core).wait_recv()
-
-        @pl.when(step == far)
-        def _():
+            for way in (0, 1):
+                device = chip_at(way, near) * 2 + core
+                slot = lax.broadcasted_iota(jnp.int32, (FAR_STEPS * tile, rows), 0)
+                onward = slot // tile + 1
+                chip = (z + onward) % chips if way == 0 else (z + chips - onward) % chips
+                want = ((chip * 2 + slot % tile // slots) * slots + slot % slots).astype(F32)
+                c_out[way] = jnp.dot(
+                    picks(info[device], want), rows_at(device), preferred_element_type=F32
+                ).astype(BF16)
+                for piece in (0, 1):
+                    c_copy(way, 0, piece).start()
+
+    def far_arrivals(number):
+        for way in (0, 1):
+            for piece in pieces_of(number):
+                c_copy(way, number, piece).wait_recv()
+            if number + 1 < FAR_STEPS:
+                for piece in pieces_of(number + 1):
+                    c_copy(way, number + 1, piece).start()
+            cm_copy(way, number).start()
+
+    def arrive(step):
+        pl.when(step <= near)(functools.partial(near_arrivals, step))
+        for number in range(FAR_STEPS):
+            pl.when(step == near + 1 + number)(functools.partial(far_arrivals, number))
+
+    def select_near(step):
+        for way in (0, 1):
             for sub in (0, 1):
-                m2_copy(0, 0, sub, 1 - core).wait_recv()
-
-        near = jnp.where(step == far, z, chip_at(0, step))
+                m2_copy(way, step, sub, 1 - core).wait_recv()
         total = None
-        for number, (chip, owner) in enumerate(
-            ((near, 0), (chip_at(1, step), 0), (near, 1), (chip_at(1, step), 1))
-        ):
-            device = chip * 2 + owner
-            table = info[device]
-            slot = lax.broadcasted_iota(jnp.int32, (4 * slots, rows), 0)
+        for number, (way, owner) in enumerate(((0, 0), (1, 0), (0, 1), (1, 1))):
+            device = chip_at(way, step) * 2 + owner
+            slot = lax.broadcasted_iota(jnp.int32, (2 * tile, rows), 0)
             want = jnp.where(slot // slots == number, sp * slots + slot % slots, -2).astype(F32)
-            hit = jnp.logical_or(table[0:1, 0:rows] == want, table[1:2, 0:rows] == want)
-            block = rows_buf[pl.ds(pl.multiple_of(device * rows, rows), rows)]
             picked = jnp.dot(
-                jnp.where(hit, 1.0, 0.0).astype(BF16), block, preferred_element_type=F32
+                picks(info[device], want), rows_at(device), preferred_element_type=F32
             )
             total = picked if total is None else total + picked
-        x_buf[pair, tp] = total.astype(BF16)
+        x_buf[step, tp] = total.astype(BF16)
+        for way in (0, 1):
+            a_near(way, step, tp).start()
+
+    def my_half(ref, at):
+        both = ref[at].astype(F32)
+        return jnp.where(core == 0, both[0:slots], both[slots:tile])
+
+    def select_far(step):
+        pair = step % far
+        for number in range(FAR_STEPS):
+
+            @pl.when(step == near + 1 + number)
+            def _(number=number):
+                for way in (0, 1):
+                    cm_copy(way, number).wait_recv()
+                for owner in (0, 1):
+                    if owner == 0:
+                        at_row = core * tile
+                        source, at = c_in, slice(number * tile, (number + 1) * tile)
+                    else:
+                        at_row = (1 - core) * tile
+                        source, at = c_mate, slice(None)
+                    if number < FAR_STEPS - 1:
+                        low = my_half(source, (0, number, at))
+                        high = my_half(source, (1, number, at))
+                    else:
+                        low = own_rows[owner]
+                        high = jnp.concatenate(
+                            [
+                                my_half(source, (0, number, at, slice(0, cols))),
+                                my_half(source, (1, number, at, slice(cols, 2 * cols))),
+                            ],
+                            axis=1,
+                        )
+                    x_buf[pair, tp, pl.ds(pl.multiple_of(at_row, tile), tile)] = jnp.concatenate(
+                        [low, high], axis=0
+                    ).astype(BF16)
+
         for way in (0, 1):
             a_near(way, pair, tp).start()
+
+    slot8 = lax.broadcasted_iota(jnp.int32, (slots, rows), 0)
+    own_want = (sp * slots + slot8).astype(F32)
+    own_rows[0] = jnp.dot(picks(info[sp], own_want), normed, preferred_element_type=F32)
+    for sub in (0, 1):
+        m2_copy(0, 0, sub, 1 - core).wait_recv()
+    other = z * 2 + (1 - core)
+    own_rows[1] = jnp.dot(picks(info[other], own_want), rows_at(other), preferred_element_type=F32)
 
     def forward(step):
         pair = step % far
@@ -582,33 +686,69 @@
         e_buf[pair] = total.astype(BF16).reshape(2, 2 * slots, 2 * cols)
         e_copy(pair).start()
 
-    stages = (ring_arrivals, select, forward, run_expert)
+    stages = (
+        (0, arrive, 1, far),
+        (1, forward, 1, far),
+        (0, select_far, near + 1, far),
+        (2, run_expert, 1, far),
+        (0, select_near, 1, near),
+    )
 
     def tick(at, nothing):
-        for lag, stage in enumerate(stages):
+        for lag, stage, first, last in stages:
             step = at - lag
-            pl.when(jnp.logical_and(step >= 1, step <= far))(functools.partial(stage, step))
+            pl.when(jnp.logical_and(step >= first, step <= last))(functools.partial(stage, step))
         return nothing
 
-    lax.fori_loop(1, far + len(stages), tick, 0)
-
-    def contribution(chip, pair, which, sub):
+    lax.fori_loop(1, far + 3, tick, 0)
+
+    def weighted(chip, want, stack):
         table = info[chip * 2 + core]
-        slot = lax.broadcasted_iota(jnp.int32, (4 * slots, rows), 0)
-        expert = jnp.where(slot < 2 * slots, sp, z * 2 + (1 - core))
-        ours = (slot % (2 * slots)) // slots == which
-        want = jnp.where(ours, expert * slots + slot % slots, -2).astype(F32)
         weight = jnp.where(table[0:1, 0:rows] == want, table[2:3, 0:rows], 0.0)
         weight = weight + jnp.where(table[1:2, 0:rows] == want, table[3:4, 0:rows], 0.0)
         coarse = weight.astype(BF16)
         fine = (weight - coarse.astype(F32)).astype(BF16)
-        at = slice(sub * cols, (sub + 1) * cols)
-        mine, other = e_buf[pair, core, :, at], e_mate[pair, :, at]
         return lax.dot_general(
             jnp.concatenate([coarse, fine], axis=0),
-            jnp.concatenate([mine, other, mine, other], axis=0),
+            jnp.concatenate([stack, stack], axis=0),
             (((0,), (0,)), ((), ())),
             preferred_element_type=F32,
+        )
+
+    def contribution(chip, pair, which, sub):
+        slot = lax.broadcasted_iota(jnp.int32, (2 * tile, rows), 0)
+        expert = jnp.where(slot < tile, sp, z * 2 + (1 - core))
+        ours = (slot % tile) // slots == which
+        want = jnp.where(ours, expert * slots + slot % slots, -2).astype(F32)
+        at = slice(sub * cols, (sub + 1) * cols)
+        return weighted(
+            chip, want, jnp.concatenate([e_buf[pair, core, :, at], e_mate[pair, :, at]], axis=0)
+        )
+
+    def passed_on(way, sub):
+        chip = chip_at(1 - way, near)
+        slot = lax.broadcasted_iota(jnp.int32, (FAR_STEPS * tile, rows), 0)
+        giver = chip_at(way, FAR_STEPS - slot // tile)
+        want = ((giver * 2 + slot % tile // slots) * slots + slot % slots).astype(F32)
+        at = slice(sub * cols, (sub + 1) * cols)
+        return weighted(chip, want, g_in[way, FAR_STEPS - 1, :, at])
+
+    def g_copy(way, number, piece):
+        at = (pl.ds(piece * tile, tile),)
+        to = ()
+        if piece == 0:
+            at = at + (pl.ds(way * cols, cols),)
+            to = (slice(None), pl.ds(way * cols, cols))
+        if piece == number:
+            src = g_out.at[(way, number) + to]
+        else:
+            src = g_in.at[(way, number - 1) + at]
+        return hop(
+            src,
+            g_in.at[(way, number) + at],
+            gsend.at[way, number, piece],
+            grecv.at[way, number, piece],
+            along(way),
         )
 
     def r_copy(way, step, sub):
@@ -623,24 +763,43 @@
 
     for way in (0, 1):
         rest = slice((1 - way) * cols, (2 - way) * cols)
-        ret_in[way, 0, :, rest] = jnp.zeros((rows, cols), BF16)
-
-    def start_back():
-        for way in (0, 1):
-            at = slice(way * cols, (way + 1) * cols)
-            ret_out[way, 0, :, at] = contribution((z + far) % chips, 0, 1, way).astype(BF16)
-            r_copy(way, 0, way).start()
-
-    def go_back(distance):
+        g_in[way, FAR_STEPS - 1, 0:tile, rest] = jnp.zeros((tile, cols), BF16)
+
+    def far_back(number):
+        pair = (far - number) % far
+        for way in (0, 1):
+            for piece in range(number):
+                g_copy(way, number - 1, piece).wait_recv()
+                g_copy(way, number, piece).start()
+        e_copy(pair).wait_recv()
+        for way in (0, 1):
+            which = 1 if number == 0 else 1 - way
+            at = slice(which * slots, (which + 1) * slots)
+            mine = e_buf[pair, core].astype(F32)[at]
+            other = e_mate[pair].astype(F32)[at]
+            g_out[way, number] = jnp.concatenate(
+                [jnp.where(core == 0, mine, other), jnp.where(core == 0, other, mine)], axis=0
+            ).astype(BF16)
+            g_copy(way, number, number).start()
+
+    def near_back(distance):
         step = far - distance
+        e_copy(distance).wait_recv()
+
+        @pl.when(distance == near)
+        def _():
+            for way in (0, 1):
+                for piece in range(FAR_STEPS):
+                    g_copy(way, FAR_STEPS - 1, piece).wait_recv()
+                for sub in (0, 1):
+                    at = slice(sub * cols, (sub + 1) * cols)
+                    ret_in[way, FAR_STEPS - 1, :, at] = passed_on(way, sub).astype(BF16)
+
         for turn in (0, 1):
             for way in (0, 1):
                 sub = turn if way == 0 else 1 - turn
                 added = contribution(chip_at(1 - way, distance), distance, 1 - way, sub)
-                if turn == 0:
-                    r_copy(way, step - 1, sub).wait_recv()
-                else:
-                    pl.when(step > 1)(lambda: r_copy(way, step - 1, sub).wait_recv())
+                pl.when(distance < near)(lambda: r_copy(way, step - 1, sub).wait_recv())
                 at = slice(sub * cols, (sub + 1) * cols)
                 ret_out[way, step, :, at] = (
                     added + ret_in[way, step - 1, :, at].astype(F32)
@@ -648,9 +807,9 @@
                 r_copy(way, step, sub).start()
 
     def back(distance):
-        e_copy(distance % far).wait_recv()
-        pl.when(distance == far)(start_back)
-        pl.when(distance < far)(functools.partial(go_back, distance))
+        for number in range(FAR_STEPS):
+            pl.when(distance == far - number)(functools.partial(far_back, number))
+        pl.when(distance <= near)(functools.partial(near_back, distance))
 
     back_stages = ((2, back), (1, finish), (0, add_far), (-2, begin_sum))
 
@@ -685,20 +844,29 @@
             for sub in (0, 1):
                 z_copy(way, step, sub).wait_send()
                 m_copy(way, step, sub, core).wait_send()
+        return nothing
+
+    def drain_near(step, nothing):
+        for way in (0, 1):
+            for sub in (0, 1):
                 z2_copy(way, step, sub).wait_send()
                 m2_copy(way, step, sub, core).wait_send()
-                r_copy(way, step, sub).wait_send()
+                r_copy(way, far - step, sub).wait_send()
         return nothing
 
     lax.fori_loop(1, far, drain, 0)
+    lax.fori_loop(1, near + 1, drain_near, 0)
     i_copy(0, far).wait_send()
     im_copy(0, far, core).wait_send()
     for way in (0, 1):
         z_copy(way, far, way).wait_send()
         m_copy(way, far, way, core).wait_send()
-        z2_copy(way, far, way).wait_send()
-        m2_copy(way, far, way, core).wait_send()
-        r_copy(way, 0, way).wait_send()
+        for number in range(FAR_STEPS):
+            for piece in pieces_of(number):
+                c_copy(way, number, piece).wait_send()
+            cm_copy(way, number).wait_send()
+            for piece in range(number + 1):
+                g_copy(way, number, piece).wait_send()
 
     def drain_pairs(pair, nothing):
         e_copy(pair).wait_send()
@@ -771,6 +939,12 @@
             pltpu.VMEM((far, picked // 2, width), BF16),
             pltpu.VMEM((2, far, rows, width), BF16),
             pltpu.VMEM((2, far, rows, width), BF16),
+            pltpu.VMEM((2, FAR_STEPS * picked // 2, width), BF16),
+            pltpu.VMEM((2, FAR_STEPS, FAR_STEPS * picked // 2, width), BF16),
+            pltpu.VMEM((2, FAR_STEPS, picked // 2, width), BF16),
+            pltpu.VMEM((2, picked // 4, width), F32),
+            pltpu.VMEM((2, FAR_STEPS, picked // 2, width), BF16),
+            pltpu.VMEM((2, FAR_STEPS, FAR_STEPS * picked // 2, width), BF16),
             dma((5,)),
             dma((2, far, 2)),
             dma((2, far, 2)),
@@ -794,6 +968,12 @@
             dma((far,)),
             dma((2, far, 2)),
             dma((2, far, 2)),
+            dma((2, FAR_STEPS, 2)),
+            dma((2, FAR_STEPS, 2)),
+            dma((2, FAR_STEPS)),
+            dma((2, FAR_STEPS)),
+            dma((2, FAR_STEPS, FAR_STEPS)),
+            dma((2, FAR_STEPS, FAR_STEPS)),
         ],
         compiler_params=pltpu.CompilerParams(
             collective_id=0, has_side_effects=True, vmem_limit_bytes=64 * 1024 * 1024 - 65536

time: 208 us -> 212 us (1.019)
  Pallas kernels: 202 us -> 205 us
    pallas_call x1, Pallas kernels: 202 us -> 205 us  [layer(): pl.pallas_call(functools.partial(layer_kernel, chips, peers), out_shape=j...]
where the time goes in v4:
time: 212 us
  Pallas kernels  205 us (97%)
  other arithmetic  3.59 us (2%)
  local copies, waits for them, and re-layouts  2.85 us (1%)
    pallas_call x1, Pallas kernels, layer(): pl.pallas_call(functools.partial(layer_kernel, chips, peers), out_shape=j...  205 us

profile of v4, /device:TPU:33, one launch (start us, length us, event | category | flops | bytes accessed | tf_op | source)
XLA Modules:
  0.0 212.1 jit_solution(4456681564800180225)
XLA Ops:
  0.0 0.0 copy-start.4
  0.0 0.0 copy-start.5
  0.0 0.0 copy-start.7
  0.0 0.0 copy-start.6
  0.0 0.0 copy-start
  0.0 0.0 copy-start.1
  0.0 0.0 copy-start.2
  0.0 0.0 copy-start.3
  0.1 0.1 multiply_bitcast_fusion
  0.2 0.3 concatenate.64
  0.6 0.5 fusion.4
  1.1 0.1 multiply_bitcast_fusion.3
  1.2 0.6 fusion
  1.8 0.8 pad_maximum_fusion.tables_ref
  2.6 0.0 copy-done.4
  2.6 0.0 copy-done.5
  2.6 0.1 maximum_bitcast_fusion.1
  2.7 0.0 copy-done.7
  2.7 0.0 copy-done.6
  2.7 0.6 pad_maximum_fusion.3.gains_ref
  3.3 0.0 copy-done
  3.3 0.1 copy.20
  3.4 0.0 copy-done.1
  3.4 0.1 copy.21
  3.5 0.7 pad_maximum_fusion.2.kvn_ref
  4.3 0.0 copy-done.2
  4.3 0.0 copy-done.3
  4.3 0.6 pad.4.route_ref
  4.9 205.5 %layer.1 = bf16[64,2048]{1,0:T(8,128)(2,1)} custom-call(bf16[256,256]{1,0:T(8,128)(2,1)} %qw_ref.1, bf16[256,128]{1,0:T(8,128)(2,1)} %kw_ref.1, bf16[256,128]{1,0:T(8,128)(2,1)} %vw_ref.1, bf16[256,128]{1,0:T(8,128)(2,1)} %qn_ref.1, bf16[256,128]{1,0:T(8,128)(2,1)} %pad_maximum_fusion.2.kvn_ref, f32[4,128]{1,0:T(4,128)} %pad_maximum_fusion.3.gains_ref, ...), custom_call_target="tpu_custom_call" | custom-call | tf_op jit(solution)/shard_map/layer/pallas_call | solution.py:910
  210.4 1.7 copy.23
  (7 shorter events, 0.1 us)
Async XLA Ops:
  0.0 2.6 %copy-start.4 = (f32[64]{0:T(128)S(1)}, f32[64]{0:T(128)}, u32[]{:S(2)}) copy-start(f32[64]{0:T(128)} %param.28) | copy-start | bytes 772
  0.0 2.6 %copy-start.5 = (f32[64]{0:T(128)S(1)}, f32[64]{0:T(128)}, u32[]{:S(2)}) copy-start(f32[64]{0:T(128)} %param.29) | copy-start | bytes 772
  0.0 2.7 %copy-start.7 = (f32[128]{0:T(128)S(1)}, f32[128]{0:T(128)}, u32[]{:S(2)}) copy-start(f32[128]{0:T(128)} %param.26) | copy-start | bytes 1540
  0.0 2.7 %copy-start.6 = (f32[128]{0:T(128)S(1)}, f32[128]{0:T(128)}, u32[]{:S(2)}) copy-start(f32[128]{0:T(128)} %param.27) | copy-start | bytes 1540
  0.0 3.3 %copy-start = (bf16[256,64]{0,1:T(8,128)(2,1)S(1)}, bf16[256,64]{0,1:T(8,128)(2,1)}, u32[]{:S(2)}) copy-start(bf16[256,64]{0,1:T(8,128)(2,1)} %param.24) | copy-start | bytes 98308
  0.0 3.4 %copy-start.1 = (bf16[256,64]{0,1:T(8,128)(2,1)S(1)}, bf16[256,64]{0,1:T(8,128)(2,1)}, u32[]{:S(2)}) copy-start(bf16[256,64]{0,1:T(8,128)(2,1)} %param.25) | copy-start | bytes 98308
  0.0 4.2 %copy-start.2 = (s32[64,2]{0,1:T(2,128)S(1)}, s32[64,2]{0,1:T(2,128)}, u32[]{:S(2)}) copy-start(s32[64,2]{0,1:T(2,128)} %param.36) | copy-start | bytes 1540
  0.0 4.2 %copy-start.3 = (f32[64,2]{0,1:T(2,128)S(1)}, f32[64,2]{0,1:T(2,128)}, u32[]{:S(2)}) copy-start(f32[64,2]{0,1:T(2,128)} %param.37) | copy-start | bytes 1540

commit v5 on v4

--- a/solution.py
+++ b/solution.py
@@ -688,10 +688,11 @@
 
     stages = (
         (0, arrive, 1, far),
-        (1, forward, 1, far),
-        (0, select_far, near + 1, far),
-        (2, run_expert, 1, far),
-        (0, select_near, 1, near),
+        (1, select_near, 1, near),
+        (1, select_far, near + 1, far - 1),
+        (0, select_far, far, far),
+        (2, forward, 1, far),
+        (3, run_expert, 1, far),
     )
 
     def tick(at, nothing):
@@ -700,7 +701,7 @@
             pl.when(jnp.logical_and(step >= first, step <= last))(functools.partial(stage, step))
         return nothing
 
-    lax.fori_loop(1, far + 3, tick, 0)
+    lax.fori_loop(1, far + 4, tick, 0)
 
     def weighted(chip, want, stack):
         table = info[chip * 2 + core]
@@ -811,7 +812,7 @@
             pl.when(distance == far - number)(functools.partial(far_back, number))
         pl.when(distance <= near)(functools.partial(near_back, distance))
 
-    back_stages = ((2, back), (1, finish), (0, add_far), (-2, begin_sum))
+    back_stages = ((3, back), (2, finish), (0, add_far), (-2, begin_sum))
 
     def back_tick(at, nothing):
         for lag, stage in back_stages:
@@ -820,7 +821,7 @@
             pl.when(jnp.logical_and(step >= 1, step <= last))(functools.partial(stage, step))
         return nothing
 
-    lax.fori_loop(0, far + 2, back_tick, 0)
+    lax.fori_loop(0, far + 3, back_tick, 0)
     for sub in (0, 1):
         at = slice(sub * cols, (sub + 1) * cols)
         total = att_buf[:, at].astype(F32) + contribution(z, 0, 0, sub)

time: 212 us -> 208 us (0.981)
  Pallas kernels: 205 us -> 201 us
    pallas_call x1, Pallas kernels: 205 us -> 201 us  [layer(): pl.pallas_call(functools.partial(layer_kernel, chips, peers), out_shape=j...]
where the time goes in v5:
time: 208 us
  Pallas kernels  201 us (97%)
  other arithmetic  3.59 us (2%)
  local copies, waits for them, and re-layouts  2.85 us (1%)
    pallas_call x1, Pallas kernels, layer(): pl.pallas_call(functools.partial(layer_kernel, chips, peers), out_shape=j...  201 us

profile of v5, /device:TPU:33, one launch (start us, length us, event | category | flops | bytes accessed | tf_op | source)
XLA Modules:
  0.0 207.7 jit_solution(15856045617110334444)
XLA Ops:
  0.0 0.0 copy-start.4
  0.0 0.0 copy-start.5
  0.0 0.0 copy-start.7
  0.0 0.0 copy-start.6
  0.0 0.0 copy-start
  0.0 0.0 copy-start.1
  0.0 0.0 copy-start.2
  0.0 0.0 copy-start.3
  0.1 0.1 multiply_bitcast_fusion
  0.2 0.3 concatenate.64
  0.6 0.5 fusion.4
  1.1 0.1 multiply_bitcast_fusion.3
  1.2 0.6 fusion
  1.8 0.8 pad_maximum_fusion.tables_ref
  2.6 0.0 copy-done.4
  2.6 0.0 copy-done.5
  2.6 0.1 maximum_bitcast_fusion.1
  2.7 0.0 copy-done.7
  2.7 0.0 copy-done.6
  2.7 0.6 pad_maximum_fusion.3.gains_ref
  3.3 0.0 copy-done
  3.3 0.1 copy.20
  3.4 0.0 copy-done.1
  3.4 0.1 copy.21
  3.5 0.7 pad_maximum_fusion.2.kvn_ref
  4.3 0.0 copy-done.2
  4.3 0.0 copy-done.3
  4.3 0.6 pad.4.route_ref
  4.9 201.1 %layer.1 = bf16[64,2048]{1,0:T(8,128)(2,1)} custom-call(bf16[256,256]{1,0:T(8,128)(2,1)} %qw_ref.1, bf16[256,128]{1,0:T(8,128)(2,1)} %kw_ref.1, bf16[256,128]{1,0:T(8,128)(2,1)} %vw_ref.1, bf16[256,128]{1,0:T(8,128)(2,1)} %qn_ref.1, bf16[256,128]{1,0:T(8,128)(2,1)} %pad_maximum_fusion.2.kvn_ref, f32[4,128]{1,0:T(4,128)} %pad_maximum_fusion.3.gains_ref, ...), custom_call_target="tpu_custom_call" | custom-call | tf_op jit(solution)/shard_map/layer/pallas_call | solution.py:911
  206.1 1.7 copy.23
  (7 shorter events, 0.1 us)
Async XLA Ops:
  0.0 2.6 %copy-start.4 = (f32[64]{0:T(128)S(1)}, f32[64]{0:T(128)}, u32[]{:S(2)}) copy-start(f32[64]{0:T(128)} %param.28) | copy-start | bytes 772
  0.0 2.6 %copy-start.5 = (f32[64]{0:T(128)S(1)}, f32[64]{0:T(128)}, u32[]{:S(2)}) copy-start(f32[64]{0:T(128)} %param.29) | copy-start | bytes 772
  0.0 2.7 %copy-start.7 = (f32[128]{0:T(128)S(1)}, f32[128]{0:T(128)}, u32[]{:S(2)}) copy-start(f32[128]{0:T(128)} %param.26) | copy-start | bytes 1540
  0.0 2.7 %copy-start.6 = (f32[128]{0:T(128)S(1)}, f32[128]{0:T(128)}, u32[]{:S(2)}) copy-start(f32[128]{0:T(128)} %param.27) | copy-start | bytes 1540
  0.0 3.3 %copy-start = (bf16[256,64]{0,1:T(8,128)(2,1)S(1)}, bf16[256,64]{0,1:T(8,128)(2,1)}, u32[]{:S(2)}) copy-start(bf16[256,64]{0,1:T(8,128)(2,1)} %param.24) | copy-start | bytes 98308
  0.0 3.4 %copy-start.1 = (bf16[256,64]{0,1:T(8,128)(2,1)S(1)}, bf16[256,64]{0,1:T(8,128)(2,1)}, u32[]{:S(2)}) copy-start(bf16[256,64]{0,1:T(8,128)(2,1)} %param.25) | copy-start | bytes 98308
  0.0 4.2 %copy-start.2 = (s32[64,2]{0,1:T(2,128)S(1)}, s32[64,2]{0,1:T(2,128)}, u32[]{:S(2)}) copy-start(s32[64,2]{0,1:T(2,128)} %param.36) | copy-start | bytes 1540
  0.0 4.2 %copy-start.3 = (f32[64,2]{0,1:T(2,128)S(1)}, f32[64,2]{0,1:T(2,128)}, u32[]{:S(2)}) copy-start(f32[64,2]{0,1:T(2,128)} %param.37) | copy-start | bytes 1540

commit v6 on v5

--- a/solution.py
+++ b/solution.py
@@ -69,9 +69,16 @@
     kw_ref,
     vw_ref,
     qn_ref,
-    kvn_ref,
-    gains_ref,
-    tables_ref,
+    kn_ref,
+    vn_ref,
+    gain_qw,
+    gain_kw,
+    gain_qn,
+    gain_kn,
+    cos_w_ref,
+    sin_w_ref,
+    cos_n_ref,
+    sin_n_ref,
     res_ref,
     norm_gain_ref,
     route_ref,
@@ -174,12 +181,16 @@
         at = pl.multiple_of((chip * 2 + owner) * tok + sub * half, half)
         return kv_buf.at[pl.ds(at, half)]
 
-    cos_w, sin_w = tables_ref[0], tables_ref[1]
-    cos_n, sin_n = tables_ref[2], tables_ref[3]
+    cos_w, sin_w = cos_w_ref[...], sin_w_ref[...]
+    cos_n, sin_n = cos_n_ref[...], sin_n_ref[...]
+
+    def beside_itself(ref):
+        return jnp.concatenate([ref[...], ref[...]], axis=1)
+
     own = pl.ds(pl.multiple_of(sp * tok, tok), tok)
-    k_wide = rotate(norm_wide(kw_ref[...].astype(F32), gains_ref[1:2]), cos_w, sin_w, wide // 4)
-    kvn = kvn_ref[...].astype(F32)
-    k_narrow = rotate(norm_halves(kvn, gains_ref[3:4]), cos_n, sin_n, wide // 8)
+    k_wide = rotate(norm_wide(kw_ref[...].astype(F32), gain_kw[...]), cos_w, sin_w, wide // 4)
+    kvn = jnp.concatenate([kn_ref[...].astype(F32), vn_ref[...].astype(F32)], axis=1)
+    k_narrow = rotate(norm_halves(kvn, beside_itself(gain_kn)), cos_n, sin_n, wide // 8)
     kv_buf[own, 0:wide] = k_wide.astype(BF16)
     kv_buf[own, wide : 2 * wide] = vw_ref[...]
     kv_buf[own, 2 * wide : 3 * wide] = jnp.where(
@@ -257,9 +268,9 @@
 
     qw = qw_ref[...].astype(F32)
     for head in (0, 1):
-        q = norm_wide(qw[:, head * wide : (head + 1) * wide], gains_ref[0:1])
+        q = norm_wide(qw[:, head * wide : (head + 1) * wide], gain_qw[...])
         qws[head * tok : (head + 1) * tok] = rotate(q, cos_w, sin_w, wide // 4).astype(BF16)
-    qn = rotate(norm_halves(qn_ref[...].astype(F32), gains_ref[2:3]), cos_n, sin_n, wide // 8)
+    qn = rotate(norm_halves(qn_ref[...].astype(F32), beside_itself(gain_qn)), cos_n, sin_n, wide // 8)
     low = lane_ids(qn.shape) < wide // 2
     qns[0:tok] = jnp.where(low, qn, 0.0).astype(BF16)
     qns[tok : 2 * tok] = jnp.where(low, pltpu.roll(qn, wide // 2, 1), 0.0).astype(BF16)
@@ -688,11 +699,10 @@
 
     stages = (
         (0, arrive, 1, far),
-        (1, select_near, 1, near),
-        (1, select_far, near + 1, far - 1),
-        (0, select_far, far, far),
-        (2, forward, 1, far),
         (3, run_expert, 1, far),
+        (0, select_near, 1, near),
+        (0, select_far, near + 1, far),
+        (1, forward, 1, far),
     )
 
     def tick(at, nothing):
@@ -911,7 +921,7 @@
     return pl.pallas_call(
         functools.partial(layer_kernel, chips, peers),
         out_shape=jax.ShapeDtypeStruct((rows, width), BF16),
-        in_specs=[vmem] * 10 + [hbm] * 5,
+        in_specs=[vmem] * 17 + [hbm] * 5,
         out_specs=vmem,
         scratch_shapes=[
             pltpu.VMEM((2 * chips * tok, 3 * wide), BF16),
@@ -985,9 +995,10 @@
         keys_wide,
         values_wide,
         queries_narrow,
-        jnp.concatenate([keys_narrow, values_narrow], axis=1),
-        gains,
-        tables,
+        keys_narrow,
+        values_narrow,
+        *gains,
+        *tables,
         residual,
         norm_gain.reshape(1, width),
         route,
@@ -1030,21 +1041,15 @@
     lanes = jnp.arange(wide_width, dtype=jnp.int32)
     wide_sign = jnp.where(lanes % (wide_width // 2) < wide_width // 4, -1.0, 1.0)
     narrow_sign = jnp.where(lanes % (narrow_width // 2) < narrow_width // 4, -1.0, 1.0)
-    tables = jnp.stack(
-        [
-            jnp.cos(wide_angles),
-            jnp.sin(wide_angles) * wide_sign,
-            jnp.cos(narrow_angles),
-            jnp.sin(narrow_angles) * narrow_sign,
-        ]
+    tables = (
+        jnp.cos(wide_angles),
+        jnp.sin(wide_angles) * wide_sign,
+        jnp.cos(narrow_angles),
+        jnp.sin(narrow_angles) * narrow_sign,
     )
-    gains = jnp.stack(
-        [
-            query_gain_wide,
-            key_gain_wide,
-            jnp.concatenate([query_gain_narrow, query_gain_narrow]),
-            jnp.concatenate([key_gain_narrow, key_gain_narrow]),
-        ]
+    gains = tuple(
+        gain.reshape(1, -1)
+        for gain in (query_gain_wide, key_gain_wide, query_gain_narrow, key_gain_narrow)
     )
     own_rows = residual.shape[0]
     route = jnp.concatenate([route_ids.astype(F32), route_weights], axis=1).T

time: 208 us -> 207 us (level)
  Pallas kernels: 201 us -> 196 us
  local copies, waits for them, and re-layouts: 2.85 us -> 5.56 us
    pallas_call x1, Pallas kernels: 201 us -> 196 us  [layer(): pl.pallas_call(functools.partial(layer_kernel, chips, peers), out_shape=j...]
    mul x0 -> x4, other arithmetic: none -> 2.72 us  [the longest x1 1.27 us: body(): jnp.sin(wide_angles) * wide_sign]
    unnamed x19 -> x3, local copies, waits for them, and re-layouts: 1.93 us -> 4.65 us
where the time goes in v6:
time: 207 us; the launch traced here: 206 us
  Pallas kernels  196 us (95%)
  local copies, waits for them, and re-layouts  5.56 us (3%)
  other arithmetic  4.13 us (2%)
    pallas_call x1, Pallas kernels, layer(): pl.pallas_call(functools.partial(layer_kernel, chips, peers), out_shape=j...  196 us
    unnamed x3, local copies, waits for them, and re-layouts  4.65 us

profile of v6, /device:TPU:33, one launch (start us, length us, event | category | flops | bytes accessed | tf_op | source)
XLA Modules:
  0.0 205.9 jit_solution(10876555319382991300)
XLA Ops:
  0.0 0.1 broadcast_multiply_fusion
  0.2 0.3 concatenate.12
  0.5 1.2 sine_multiply_fusion
  1.7 0.1 broadcast_multiply_fusion.3
  1.9 1.3 sine_multiply_fusion.1
  3.1 1.5 copy.20.kn_ref
  4.6 1.5 copy.21.vn_ref
  6.1 0.7 convert_element_type.21
  6.8 0.7 maximum_bitcast_fusion
  7.5 0.6 pad.4.route_ref
  8.1 196.1 %layer.1 = bf16[64,2048]{1,0:T(8,128)(2,1)} custom-call(bf16[256,256]{1,0:T(8,128)(2,1)} %qw_ref.1, bf16[256,128]{1,0:T(8,128)(2,1)} %kw_ref.1, bf16[256,128]{1,0:T(8,128)(2,1)} %vw_ref.1, bf16[256,128]{1,0:T(8,128)(2,1)} %qn_ref.1, bf16[256,64]{1,0:T(8,128)(2,1)} %copy.20.kn_ref, bf16[256,64]{1,0:T(8,128)(2,1)} %copy.21.vn_ref, f32[1,128]{1,0:T(1,128)} %bitcast.8, ...), custom_call_target="tpu_custom_call" | custom-call | tf_op jit(solution)/shard_map/layer/pallas_call | solution.py:921
  204.2 1.7 copy.23
  (5 shorter events, 0.0 us)

commit v7 on v6

--- a/solution.py
+++ b/solution.py
@@ -400,22 +400,23 @@
     rows = res_ref.shape[0]
     cols = res_ref.shape[1] // 2
 
-    def x_copy(way, number):
+    def x_copy(way, number, part_of):
         dest = (tp + 1) % peers if way == 0 else (tp + peers - 1) % peers
         with_far = way * cols
         alone = (1 - way) * cols
+        these = pl.ds(part_of * (rows // 2), rows // 2)
         if number == 0:
-            src = part.at[(tp + 2) % peers, :, pl.ds(with_far, cols)]
-            dst = first_in.at[way]
+            src = part.at[(tp + 2) % peers, these, pl.ds(with_far, cols)]
+            dst = first_in.at[way, these]
         else:
             at = pl.ds(alone if number == 1 else with_far, cols)
-            src = part.at[dest, :, at]
-            dst = last_in.at[way, :, at]
+            src = part.at[dest, these, at]
+            dst = last_in.at[way, these, at]
         return pltpu.make_async_remote_copy(
             src_ref=src,
             dst_ref=dst,
-            send_sem=xsend.at[way, number],
-            recv_sem=xrecv.at[way, number],
+            send_sem=xsend.at[way, number, part_of],
+            recv_sem=xrecv.at[way, number, part_of],
             device_id=xright if way == 0 else xleft,
             device_id_type=MESH,
         )
@@ -428,33 +429,46 @@
         )
         part[peer] = product.astype(BF16)
 
+    def add_and_send(part_of):
+        these = slice(part_of * (rows // 2), (part_of + 1) * (rows // 2))
+        for way in (0, 1):
+            dest = (tp + 1) % peers if way == 0 else (tp + peers - 1) % peers
+            x_copy(way, 0, part_of).wait_recv()
+            at = slice(way * cols, (way + 1) * cols)
+            part[dest, these, at] = (
+                part[dest, these, at].astype(F32) + first_in[way, these].astype(F32)
+            ).astype(BF16)
+            x_copy(way, 2, part_of).start()
+
+    def attend_rows(part_of):
+        these = slice(part_of * (rows // 2), (part_of + 1) * (rows // 2))
+        for way in (0, 1):
+            x_copy(way, 1, part_of).wait_recv()
+            x_copy(way, 2, part_of).wait_recv()
+        total = res_ref[these].astype(F32) + part[tp, these].astype(F32)
+        total = total + last_in[0, these].astype(F32) + last_in[1, these].astype(F32)
+        attended = total.astype(BF16)
+        att_buf[these] = attended
+        state = attended.astype(F32)
+        mean = jnp.mean(state * state, axis=-1, keepdims=True)
+        at = pl.multiple_of(sp * rows + part_of * (rows // 2), rows // 2)
+        rows_buf[pl.ds(at, rows // 2)] = (
+            state * lax.rsqrt(mean + EPS) * norm_gain_ref[...]
+        ).astype(BF16)
+
     project((tp + 2) % peers)
-    x_copy(0, 0).start()
-    x_copy(1, 0).start()
+    for way in (0, 1):
+        x_copy(way, 0, 0).start()
     project((tp + 1) % peers)
-    x_copy(0, 1).start()
+    x_copy(0, 1, 0).start()
     project((tp + peers - 1) % peers)
-    x_copy(1, 1).start()
+    x_copy(1, 1, 0).start()
+    for way in (0, 1):
+        x_copy(way, 0, 1).start()
     project(tp)
+    add_and_send(0)
     for way in (0, 1):
-        dest = (tp + 1) % peers if way == 0 else (tp + peers - 1) % peers
-        x_copy(way, 0).wait_recv()
-        at = slice(way * cols, (way + 1) * cols)
-        part[dest, :, at] = (
-            part[dest, :, at].astype(F32) + first_in[way].astype(F32)
-        ).astype(BF16)
-        x_copy(way, 2).start()
-    for way in (0, 1):
-        x_copy(way, 1).wait_recv()
-        x_copy(way, 2).wait_recv()
-    total = res_ref[...].astype(F32) + part[tp].astype(F32)
-    total = total + last_in[0].astype(F32) + last_in[1].astype(F32)
-    attended = total.astype(BF16)
-    att_buf[...] = attended
-    state = attended.astype(F32)
-    mean = jnp.mean(state * state, axis=-1, keepdims=True)
-    normed = (state * lax.rsqrt(mean + EPS) * norm_gain_ref[...]).astype(BF16)
-    rows_buf[pl.ds(pl.multiple_of(sp * rows, rows), rows)] = normed
+        x_copy(way, 1, 1).start()
 
     def block_of(chip, owner, sub):
         at = pl.multiple_of((chip * 2 + owner) * rows + sub * (rows // 2), rows // 2)
@@ -472,9 +486,11 @@
         ref = block_of(chip_at(way, step), owner, sub)
         return same(ref, p2send.at[way, step, sub], p2recv.at[way, step, sub], mate)
 
-    for way, sub in ((0, 0), (1, 1), (0, 1), (1, 0)):
-        z2_copy(way, 1, sub).start()
+    add_and_send(1)
     for sub in (0, 1):
+        attend_rows(sub)
+        for way in (0, 1):
+            z2_copy(way, 1, sub).start()
         m2_copy(0, 0, sub, core).start()
     for copy in w_copies[2:]:
         copy.wait()
@@ -556,7 +572,7 @@
     def near_arrivals(step):
         for turn in (0, 1):
             for way in (0, 1):
-                sub = turn if way == 0 else 1 - turn
+                sub = turn
                 z2_arrival(way, step, sub).wait_recv()
                 pl.when(step < near)(lambda: z2_copy(way, step + 1, sub).start())
                 m2_copy(way, step, sub, core).start()
@@ -646,7 +662,7 @@
 
     slot8 = lax.broadcasted_iota(jnp.int32, (slots, rows), 0)
     own_want = (sp * slots + slot8).astype(F32)
-    own_rows[0] = jnp.dot(picks(info[sp], own_want), normed, preferred_element_type=F32)
+    own_rows[0] = jnp.dot(picks(info[sp], own_want), rows_at(sp), preferred_element_type=F32)
     for sub in (0, 1):
         m2_copy(0, 0, sub, 1 - core).wait_recv()
     other = z * 2 + (1 - core)
@@ -842,7 +858,8 @@
 
     for way in (0, 1):
         for number in (0, 1, 2):
-            x_copy(way, number).wait_send()
+            for part_of in (0, 1):
+                x_copy(way, number, part_of).wait_send()
     for sub in (0, 1):
         m_copy(0, 0, sub, core).wait_send()
         m2_copy(0, 0, sub, core).wait_send()
@@ -965,8 +982,8 @@
             dma((2, far)),
             dma((2, far + 1)),
             dma((2, far + 1)),
-            dma((2, 3)),
-            dma((2, 3)),
+            dma((2, 3, 2)),
+            dma((2, 3, 2)),
             dma((2, far, 2)),
             dma((2, far, 2)),
             dma((2, far + 1, 2)),

time: 207 us -> 205 us (level)
  no operation moved by 1% of the time
where the time goes in v7:
time: 205 us; the launch traced here: 204 us
  Pallas kernels  195 us (95%)
  local copies, waits for them, and re-layouts  5.56 us (3%)
  other arithmetic  4.13 us (2%)
    pallas_call x1, Pallas kernels, layer(): pl.pallas_call(functools.partial(layer_kernel, chips, peers), out_shape=j...  195 us
    unnamed x3, local copies, waits for them, and re-layouts  4.65 us

profile of v7, /device:TPU:33, one launch (start us, length us, event | category | flops | bytes accessed | tf_op | source)
XLA Modules:
  0.0 204.3 jit_solution(16079298242735409435)
XLA Ops:
  0.0 0.1 broadcast_multiply_fusion
  0.2 0.3 concatenate.12
  0.5 1.2 sine_multiply_fusion
  1.7 0.1 broadcast_multiply_fusion.3
  1.9 1.3 sine_multiply_fusion.1
  3.1 1.5 copy.20.kn_ref
  4.6 1.5 copy.21.vn_ref
  6.1 0.7 convert_element_type.21
  6.8 0.7 maximum_bitcast_fusion
  7.5 0.6 pad.4.route_ref
  8.1 194.5 %layer.1 = bf16[64,2048]{1,0:T(8,128)(2,1)} custom-call(bf16[256,256]{1,0:T(8,128)(2,1)} %qw_ref.1, bf16[256,128]{1,0:T(8,128)(2,1)} %kw_ref.1, bf16[256,128]{1,0:T(8,128)(2,1)} %vw_ref.1, bf16[256,128]{1,0:T(8,128)(2,1)} %qn_ref.1, bf16[256,64]{1,0:T(8,128)(2,1)} %copy.20.kn_ref, bf16[256,64]{1,0:T(8,128)(2,1)} %copy.21.vn_ref, f32[1,128]{1,0:T(1,128)} %bitcast.8, ...), custom_call_target="tpu_custom_call" | custom-call | tf_op jit(solution)/shard_map/layer/pallas_call | solution.py:938
  202.6 1.7 copy.23
  (5 shorter events, 0.0 us)
